TPU v7x, 128 devices: a whole 4x4x4 slice. The times are simulated.
128 devices in a mesh: kv: 16 (over z, y), tp: 8 (over x, core).
Axes of the slice: x: 4, y: 4, z: 4, core: 2. Of those that a mesh axis runs over, the one named last changes fastest.
Arguments:
- tokens: bfloat16 [256, 4, 2048], P(None, None, ('kv', 'tp')), may hold values from -520 to 520
- input_norm_gain: bfloat16 [2048], replicated, may hold values from 0.099609375 to 1.8984375
- query_weight: bfloat16 [2048, 2048], P(None, 'kv'), may hold values from -0.125 to 0.125
- key_weight: bfloat16 [2048, 2048], P(None, 'kv'), may hold values from -0.125 to 0.125
- value_weight: bfloat16 [2048, 16, 128], P(None, 'kv', 'tp'), may hold values from -1.14904852 to 1.14904852
- output_gate_weight: bfloat16 [2048, 16, 128], P(None, 'kv', 'tp'), may hold values from -0.125 to 0.125
- strength_weight: bfloat16 [2048, 16], P(None, 'kv'), may hold values from -0.125 to 0.125
- decay_weight: bfloat16 [2048, 16], P(None, 'kv'), may hold values from -0.125 to 0.125
- head_decay_rate: float32 [16], P('kv'), may hold values from 0.005 to 1.5
- proposal_log_decay: float32 [256, 4, 16], P(None, None, 'kv'), may hold values from -0.69 to 0
- head_norm_gain: bfloat16 [128], P('tp'), may hold values from 0.099609375 to 1.8984375
- output_weight: bfloat16 [16, 128, 2048], P('kv', 'tp'), may hold values from -1.14904852 to 1.14904852
- output_norm_gain: bfloat16 [2048], P(('kv', 'tp')), may hold values from 0.099609375 to 1.8984375
- state: float32 [256, 16, 128, 128], P(None, 'kv', 'tp'), may hold values from -4.5961941 to 4.5961941
- previous_keys: bfloat16 [256, 4, 2048], P(None, None, 'kv'), may hold values from -6 to 6
- previous_values: bfloat16 [256, 4, 16, 128], P(None, None, 'kv', 'tp'), may hold values from -52 to 52
- previous_log_decay: float32 [256, 4, 16], P(None, None, 'kv'), may hold values from -0.7 to -0.02
- previous_strengths: float32 [256, 4, 16], P(None, None, 'kv'), may hold values from 0.1 to 0.9
- accepted: int32 [256], replicated, may hold values from 0 to 4
- parent: int32 [256, 4], replicated, may hold values from -1 to 2, as said below
Outputs:
- layer_out: bfloat16 [256, 4, 2048], P(None, None, ('kv', 'tp'))
- accepted_state: float32 [256, 16, 128, 128], P(None, 'kv', 'tp')
Inputs may be any that keep to these rules, and one draw needn't show every extreme that they name: parent[b, i] is -1 or a proposal index below i; -1 means that proposal i follows the accepted old proposals directly.
All inputs are finite; a program needn't handle non-finite values.
Results may differ from a plain program's by a relative error of at most 0.019.
Values may be sent and summed in bfloat16 or wider, within the bound.
A program may use at most 128 MiB of HBM per device.

v0:
```python
import functools

import jax
import jax.numpy as jnp
from jax import lax
from jax.experimental import pallas as pl
from jax.experimental.pallas import tpu as pltpu
from jax.sharding import PartitionSpec as P

EPS = 1e-06
F32 = jnp.float32
BF16 = jnp.bfloat16
MESH = pl.DeviceIdType.MESH
NT = (((1,), (1,)), ((), ()))
NN = (((1,), (0,)), ((), ()))
TN = (((0,), (0,)), ((), ()))


def dot(a, b, dims=NN):
    return lax.dot_general(a, b, dims, preferred_element_type=F32)


def iota(shape, dim):
    return lax.broadcasted_iota(jnp.int32, shape, dim)


def roll(x, shift):
    return x if shift % 128 == 0 else pltpu.roll(x, shift % 128, 1)


def row_to_column(row):
    n = row.shape[1]
    square = jnp.broadcast_to(row, (n, n))
    return jnp.sum(jnp.where(iota((n, n), 0) == iota((n, n), 1), square, 0.0), axis=1, keepdims=True)


def ungroup(parts, j):
    chunk = iota(parts[0].shape, 1) // 32
    halves = []
    for h in range(2):
        total = None
        for m in range(4):
            x = roll(parts[h * 4 + m], (m - j) * 32)
            total = x if total is None else jnp.where(chunk == m, x, total)
        halves.append(total)
    return jnp.concatenate(halves, axis=1)


def regroup(rows, g):
    h, m = divmod(g, 4)
    total = None
    for j in range(4):
        x = roll(rows[j][:, h * 128 : h * 128 + 128], (j - m) * 32)
        total = x if total is None else jnp.where(iota(x.shape, 1) // 32 == j, x, total)
    return total


def pick_rows(product):
    lanes = product.shape[1]
    cube = product.reshape(32, 16, lanes)
    keep = iota(cube.shape, 0) == iota(cube.shape, 2) % 32
    return jnp.sum(jnp.where(keep, cube, 0.0), axis=0)


def pick_pairs(product):
    n, lanes = product.shape[0] // 32, product.shape[1]
    cube = product.reshape(n, 32, lanes)
    keep = iota(cube.shape, 1) == iota(cube.shape, 2) % 32
    return jnp.sum(jnp.where(keep, cube, 0.0), axis=1)


def sum_of(terms):
    return functools.reduce(lambda a, b: a + b, terms)


def old_part(state, keys, old_values, log_decay, strengths, accepted, store):
    source, target = iota((128, 128), 1), iota((128, 128), 0)
    order = (source == (target % 32) * 4 + target // 32).astype(BF16)
    grouped, reads, grams = [], [], []
    for g in range(8):
        kg = dot(order, keys(g)).astype(BF16)
        grouped.append(kg)
        reads.append(pick_rows(dot(state(g).astype(BF16), kg, NT)))
        grams.append(pick_pairs(dot(kg, kg, NT)))
    gram = [ungroup(grams, j) for j in range(4)]
    read = [ungroup(reads, j) for j in range(4)]
    inv = [lax.rsqrt(gram[j][j : j + 1] + EPS) for j in range(4)]
    gam, beta = [], []
    for j in range(4):
        live = (j < accepted).astype(F32)
        g_j = log_decay[j] * live
        gam.append(g_j if j == 0 else gam[-1] + g_j)
        beta.append(strengths[j] * live)
    update = []
    for i in range(4):
        u = beta[i] * (old_values[i] - (jnp.exp(gam[i]) * inv[i]) * read[i])
        for j in range(i):
            a = beta[i] * (gram[j][i : i + 1] * (inv[i] * inv[j])) * jnp.exp(gam[i] - gam[j])
            u = u - a * update[j]
        update.append(u)
    weighted = [update[j] * (jnp.exp(gam[3] - gam[j]) * inv[j]) for j in range(4)]
    kept = jnp.exp(gam[3])
    columns = [jnp.broadcast_to(row_to_column(kept[:, h * 128 : h * 128 + 128]), (128, 128)) for h in range(2)]
    for g in range(8):
        wg = regroup(weighted, g)
        cube = (32, 16, 128)
        keep = iota(cube, 0) == iota(cube, 2) % 32
        block = jnp.where(keep, jnp.broadcast_to(wg[None], cube), 0.0).reshape(512, 128).astype(BF16)
        h, m = divmod(g, 4)
        scale = jnp.broadcast_to(columns[h][m * 32 : m * 32 + 32][:, None, :], cube).reshape(512, 128)
        store(g, scale * state(g) + dot(block, grouped[g]))


def new_part(accepted_state, query_key, values, beta_pre, decay_pre, rate, proposal, parent):
    reads, grams = [], []
    for g in range(8):
        qk = query_key(g)
        reads.append(pick_rows(dot(accepted_state(g), qk, NT)))
        grams.append(pick_pairs(dot(qk, qk, NT)))
    left = [r[:, :128] for r in reads], [r[:, 128:] for r in reads]
    aq = [ungroup(left[0], j) for j in range(4)]
    ak = [ungroup(left[1], j) for j in range(4)]
    gq = [ungroup([r[:, :128] for r in grams], j) for j in range(4)]
    gk = [ungroup([r[:, 128:] for r in grams], j) for j in range(4)]
    inv_q = [lax.rsqrt(gq[j][j : j + 1] + EPS) * (128.0**-0.5) for j in range(4)]
    inv_k = [lax.rsqrt(gk[j][4 + j : 5 + j] + EPS) for j in range(4)]
    ancestors = []
    for i in range(4):
        row = {j: (parent[i] == j).astype(F32) for j in range(i)}
        row = {j: row[j] + sum_of([jnp.zeros_like(row[j])] + [row[m] * ancestors[m][j] for m in range(j + 1, i)]) for j in range(i)}
        ancestors.append(row)
    beta, g_new, gam = [], [], []
    for i in range(4):
        x = decay_pre[i]
        softplus = jnp.maximum(x, 0.0) + jnp.log1p(jnp.exp(-jnp.abs(x)))
        g_new.append(-rate * softplus + proposal[i])
        beta.append(jax.nn.sigmoid(beta_pre[i]))
        gam.append(sum_of([g_new[i]] + [ancestors[i][j] * g_new[j] for j in range(i)]))
    outputs, update = [], []
    for i in range(4):
        grow = jnp.exp(gam[i])
        u = beta[i] * (values[i] - (grow * inv_k[i]) * ak[i])
        o = (grow * inv_q[i]) * aq[i]
        for j in range(i):
            reach = jnp.exp(jnp.minimum(gam[i] - gam[j], 0.0)) * ancestors[i][j] * inv_k[j]
            u = u - (beta[i] * inv_k[i] * gk[j][4 + i : 5 + i] * reach) * update[j]
            o = o + (inv_q[i] * gk[j][i : i + 1] * reach) * update[j]
        update.append(u)
        o = o + (inv_q[i] * gk[i][i : i + 1] * inv_k[i]) * u
        outputs.append(o)
    return outputs


def kernel(
    tp_n, kv_n,
    xt_ref, gain_ref, wq_ref, wk_ref, wv_ref, wz_ref, ws_ref, wd_ref, rate_ref, prop_ref, hgain_ref, wo_ref, ogain_ref,
    state_ref, keys_ref, oldv_ref, logd_ref, strength_ref, accepted_ref, parent_ref,
    out_ref, acc_ref,
    xall, wvz, woall, gaincol, xnorm, qkall, vzall, sdall, abf, ssq1, onorm, oall, part, racc, comb, ssq2, ssq3,
    sa, ra, sb, rb, sv, rv, sz, rz, so, ro, sq, rq, svz, rvz, ssd, rsd, sd1, rd1, se, re, sf, rf, sg, rg, sh, rh,
):
    kv, tp = lax.axis_index("kv"), lax.axis_index("tp")

    def of_tp(d):
        return lax.rem(tp + d, tp_n)

    def of_kv(d):
        return lax.rem(kv + d, kv_n)

    def copy_tp(src, dst, send, recv, d, other=None):
        return pltpu.make_async_remote_copy(
            src_ref=src, dst_ref=dst, send_sem=send.at[d], recv_sem=recv.at[d], device_id=(kv, of_tp(d)), device_id_type=MESH
        )

    def copy_kv(src, dst, send, recv, d):
        return pltpu.make_async_remote_copy(
            src_ref=src, dst_ref=dst, send_sem=send.at[d], recv_sem=recv.at[d], device_id=(of_kv(d), tp), device_id_type=MESH
        )

    barrier = pltpu.get_barrier_semaphore()
    for d in range(1, tp_n):
        pl.semaphore_signal(barrier, inc=1, device_id=(kv, of_tp(d)), device_id_type=MESH)
    for d in range(1, kv_n):
        pl.semaphore_signal(barrier, inc=1, device_id=(of_kv(d), tp), device_id_type=MESH)
    pl.semaphore_wait(barrier, tp_n - 1 + kv_n - 1)

    def tile(t):
        return t // 2, pl.ds(pl.multiple_of((t % 2) * 128, 128), 128)

    own_rows = pl.ds(pl.multiple_of((kv * tp_n + tp) * 16, 16), 16)
    pending = []
    stage_a = []
    for d in range(1, tp_n):
        p, lanes = tile(of_tp(d))
        stage_a.append(copy_tp(xt_ref.at[p, :, lanes], xall.at[own_rows], sa, ra, d))
    for c in stage_a:
        c.start()
    p, lanes = tile(tp)
    xall[own_rows, :] = xt_ref[p, :, lanes]

    stage_w = []
    for d in range(1, kv_n):
        cols = pl.ds(pl.multiple_of(of_kv(d) * 128, 128), 128)
        stage_w.append(copy_kv(wo_ref.at[:, cols], woall.at[kv], so, ro, d))
    for d in range(1, tp_n):
        stage_w.append(copy_tp(wv_ref, wvz.at[tp, 0], sv, rv, d))
        stage_w.append(copy_tp(wz_ref, wvz.at[tp, 1], sz, rz, d))
    for c in stage_w:
        c.start()
    woall[kv] = wo_ref[:, pl.ds(pl.multiple_of(kv * 128, 128), 128)]
    wvz[tp, 0] = wv_ref[...]
    wvz[tp, 1] = wz_ref[...]
    for n in range(16):
        column = row_to_column(gain_ref[:, n * 128 : n * 128 + 128].astype(F32))
        gaincol[n * 128 : n * 128 + 128, :] = jnp.broadcast_to(column, (128, 128))

    for c in stage_a:
        c.wait_recv()
    block = pl.ds(pl.multiple_of(kv * 128, 128), 128)
    stage_b = [copy_kv(xall.at[block], xall.at[block], sb, rb, d) for d in range(1, kv_n)]
    for c in stage_b:
        c.start()

    def store(g, value):
        acc_ref[g * 512 : g * 512 + 512, :] = value
        abf[g * 512 : g * 512 + 512, :] = value.astype(BF16)

    old_part(
        lambda g: state_ref[g * 512 : g * 512 + 512, :],
        lambda g: keys_ref[g * 128 : g * 128 + 128, :],
        [oldv_ref[j].astype(F32) for j in range(4)],
        [logd_ref[j] for j in range(4)],
        [strength_ref[j] for j in range(4)],
        accepted_ref[...],
        store,
    )

    for c in stage_b:
        c.wait_recv()
    squares = sum_of([jnp.sum(jnp.square(xall[n * 128 : n * 128 + 128, :].astype(F32)), axis=0, keepdims=True) for n in range(16)])
    scale = lax.rsqrt(squares / 2048.0 + EPS)
    for n in range(16):
        rows = slice(n * 128, n * 128 + 128)
        xnorm[rows, :] = (xall[rows, :].astype(F32) * scale * gaincol[rows, :]).astype(BF16)
    x = xnorm[...]
    qkall[tp, :, 0:128] = dot(x, wq_ref[...], TN).astype(BF16)
    qkall[tp, :, 128:256] = dot(x, wk_ref[...], TN).astype(BF16)
    first = iota((16, 2048), 0) == 0
    wsd = jnp.where(first, jnp.broadcast_to(ws_ref[...].astype(F32), (16, 2048)), jnp.broadcast_to(wd_ref[...].astype(F32), (16, 2048)))
    sdall[tp] = dot(wsd.astype(BF16), x)[0:8]
    stage_c = []
    for d in range(1, tp_n):
        stage_c.append(copy_tp(qkall.at[tp], qkall.at[tp], sq, rq, d))
        stage_c.append(copy_tp(sdall.at[tp], sdall.at[tp], ssd, rsd, d))
    for c in stage_c:
        c.start()
    for c in stage_w:
        c.wait_recv()
    vz = dot(wvz[...].reshape(256, 2048), x).astype(BF16)
    part_vz = vz.reshape(8, 32, 128)
    for t in range(8):
        xvz = part_vz[t]
        part[t, 0:2] = xvz.reshape(2, 16, 128)
    stage_v = []
    for d in range(1, tp_n):
        stage_v.append(copy_tp(part.at[of_tp(d), pl.ds(0, 2)], vzall.at[tp], svz, rvz, d))
    for c in stage_v:
        c.start()
    vzall[tp] = part[tp, 0:2]
    for c in stage_c + stage_v:
        c.wait_recv()

    def query_key(g):
        h, m = divmod(g, 4)
        pieces = [qkall[p * 2 + h, m * 32 : m * 32 + 32, s * 128 : s * 128 + 128] for s in range(2) for p in range(4)]
        return jnp.concatenate(pieces, axis=0)

    def both(f):
        return [jnp.concatenate([f(p * 2), f(p * 2 + 1)], axis=1) for p in range(4)]

    outputs = new_part(
        lambda g: abf[g * 512 : g * 512 + 512, :],
        query_key,
        both(lambda t: vzall[t, 0].astype(F32)),
        both(lambda t: sdall[t, 0:1, :]),
        both(lambda t: sdall[t, 1:2, :]),
        rate_ref[0],
        [prop_ref[j] for j in range(4)],
        [parent_ref[j : j + 1, :] for j in range(4)],
    )
    zgate = both(lambda t: vzall[t, 1].astype(F32))
    hgain = jnp.broadcast_to(row_to_column(hgain_ref[...].astype(F32)), (16, 256))
    sums = [jnp.sum(jnp.square(o), axis=0, keepdims=True) for o in outputs]
    for t in range(8):
        ssq1[tp, t : t + 1, :] = sums[t // 2][:, (t % 2) * 128 : (t % 2) * 128 + 128]
    stage_d = [copy_tp(ssq1.at[tp], ssq1.at[tp], sd1, rd1, d) for d in range(1, tp_n)]
    for c in stage_d:
        c.start()
    gated = [o * hgain * (z * jax.nn.sigmoid(z)) for o, z in zip(outputs, zgate)]
    for c in stage_d:
        c.wait_recv()
    scale = lax.rsqrt(jnp.sum(ssq1[...], axis=0) / 128.0 + EPS)
    for t in range(8):
        y = gated[t // 2][:, (t % 2) * 128 : (t % 2) * 128 + 128]
        onorm[t] = (y * scale[t : t + 1, :]).astype(BF16)
    stage_e = [copy_kv(onorm, oall.at[:, kv], se, re, d) for d in range(1, kv_n)]
    for c in stage_e:
        c.start()
    oall[:, kv] = onorm[...]
    weight = woall[...].reshape(256, 128)
    for c in stage_c + stage_v + stage_a + stage_b + stage_w + stage_d:
        c.wait_send()
    for c in stage_e:
        c.wait_recv()
    for t in range(8):
        product = dot(weight, oall[t].reshape(256, 128), TN)
        part[:, t] = product.astype(BF16).reshape(8, 16, 128)
    stage_f = [copy_tp(part.at[of_tp(d)], racc.at[tp], sf, rf, d) for d in range(1, tp_n)]
    for c in stage_f:
        c.start()
    racc[tp] = part[tp]
    for c in stage_f:
        c.wait_recv()
    for t in range(8):
        total = sum_of([racc[s, t].astype(F32) for s in range(8)])
        comb[t] = total
        ssq2[tp, t : t + 1, :] = jnp.sum(jnp.square(total), axis=0, keepdims=True)
    stage_g = [copy_tp(ssq2.at[tp], ssq2.at[tp], sg, rg, d) for d in range(1, tp_n)]
    for c in stage_g:
        c.start()
    for c in stage_g:
        c.wait_recv()
    ssq3[kv] = jnp.sum(ssq2[...], axis=0)
    stage_h = [copy_kv(ssq3.at[kv], ssq3.at[kv], sh, rh, d) for d in range(1, kv_n)]
    for c in stage_h:
        c.start()
    ogain = jnp.broadcast_to(row_to_column(ogain_ref[...].astype(F32)), (16, 128))
    for c in stage_h:
        c.wait_recv()
    scale = lax.rsqrt(jnp.sum(ssq3[...], axis=0) / 2048.0 + EPS)
    for t in range(8):
        out_ref[t // 2, :, (t % 2) * 128 : (t % 2) * 128 + 128] = (comb[t] * scale[t : t + 1, :] * ogain).astype(BF16)
    for c in stage_e + stage_f + stage_g + stage_h:
        c.wait_send()


def on_device(
    tokens, input_norm_gain, query_weight, key_weight, value_weight, output_gate_weight, strength_weight, decay_weight,
    head_decay_rate, proposal_log_decay, head_norm_gain, output_weight, output_norm_gain, state, previous_keys,
    previous_values, previous_log_decay, previous_strengths, accepted, parent,
):
    tp_n, kv_n = lax.axis_size("tp"), lax.axis_size("kv")
    args = [
        tokens.transpose(1, 2, 0),
        input_norm_gain.reshape(1, -1),
        query_weight,
        key_weight,
        value_weight.transpose(1, 2, 0).reshape(16, 2048),
        output_gate_weight.transpose(1, 2, 0).reshape(16, 2048),
        strength_weight.transpose(1, 0),
        decay_weight.transpose(1, 0),
        head_decay_rate,
        proposal_log_decay.transpose(1, 2, 0),
        head_norm_gain.reshape(1, 16),
        output_weight.reshape(16, 2048),
        output_norm_gain.reshape(1, 16),
        state.reshape(4096, 128),
        previous_keys.reshape(1024, 128),
        previous_values.transpose(1, 2, 3, 0).reshape(4, 16, 256),
        previous_log_decay.transpose(1, 2, 0),
        previous_strengths.transpose(1, 2, 0),
        accepted.reshape(1, 256),
        parent.transpose(1, 0),
    ]
    vmem = pl.BlockSpec(memory_space=pltpu.VMEM)
    specs = [vmem] * len(args)
    specs[8] = pl.BlockSpec(memory_space=pltpu.SMEM)

    def sems(n):
        return [pltpu.SemaphoreType.DMA((n,)), pltpu.SemaphoreType.DMA((n,))]

    out, acc = pl.pallas_call(
        functools.partial(kernel, tp_n, kv_n),
        out_shape=(jax.ShapeDtypeStruct((4, 16, 256), BF16), jax.ShapeDtypeStruct((4096, 128), F32)),
        in_specs=specs,
        out_specs=(vmem, vmem),
        scratch_shapes=[
            pltpu.VMEM((2048, 128), BF16),
            pltpu.VMEM((8, 2, 16, 2048), BF16),
            pltpu.VMEM((16, 16, 128), BF16),
            pltpu.VMEM((2048, 128), F32),
            pltpu.VMEM((2048, 128), BF16),
            pltpu.VMEM((8, 128, 256), BF16),
            pltpu.VMEM((8, 2, 16, 128), BF16),
            pltpu.VMEM((8, 8, 128), F32),
            pltpu.VMEM((4096, 128), BF16),
            pltpu.VMEM((8, 8, 128), F32),
            pltpu.VMEM((8, 16, 128), BF16),
            pltpu.VMEM((8, 16, 16, 128), BF16),
            pltpu.VMEM((8, 8, 16, 128), BF16),
            pltpu.VMEM((8, 8, 16, 128), BF16),
            pltpu.VMEM((8, 16, 128), F32),
            pltpu.VMEM((8, 8, 128), F32),
            pltpu.VMEM((16, 8, 128), F32),
            *sems(8), *sems(16), *sems(8), *sems(8), *sems(16), *sems(8), *sems(8), *sems(8), *sems(8), *sems(16), *sems(8),
            *sems(8), *sems(16),
        ],
        compiler_params=pltpu.CompilerParams(collective_id=0, has_side_effects=True, vmem_limit_bytes=48 << 20),
    )(*args)
    return out.transpose(2, 0, 1), acc.reshape(256, 1, 16, 128)


def solution(mesh):
    placed = (
        P(None, None, ("kv", "tp")),
        P(),
        P(None, "kv"),
        P(None, "kv"),
        P(None, "kv", "tp"),
        P(None, "kv", "tp"),
        P(None, "kv"),
        P(None, "kv"),
        P("kv"),
        P(None, None, "kv"),
        P("tp"),
        P("kv", "tp", None),
        P(("kv", "tp")),
        P(None, "kv", "tp", None),
        P(None, None, "kv"),
        P(None, None, "kv", "tp"),
        P(None, None, "kv"),
        P(None, None, "kv"),
        P(),
        P(),
    )
    return jax.shard_map(
        on_device,
        mesh=mesh,
        in_specs=placed,
        out_specs=(P(None, None, ("kv", "tp")), P(None, "kv", "tp", None)),
        check_vma=False,
    )
```

profile of v0, /device:TPU:1, one launch (start us, length us, event | category | flops | bytes accessed | tf_op | source)
XLA Modules:
  0.0 81.4 jit_solution(2425604401608646464)
XLA Ops:
  1.3 0.7 reshape.37.gain_ref
  2.0 0.0 copy-start
  2.0 1.6 %copy-done = f32[256,1,16,128]{3,2,1,0:T(8,128)S(1)} copy-done((f32[256,1,16,128]{3,2,1,0:T(8,128)S(1)}, f32[256,1,16,128]{3,2,1,0:T(8,128)}, u32[]{:S(2)}) %copy-start) | copy-done | bytes 2097176
  3.6 0.0 copy-start.1
  3.6 1.0 %copy-done.1 = bf16[2048,128]{1,0:T(8,128)(2,1)S(1)} copy-done((bf16[2048,128]{1,0:T(8,128)(2,1)S(1)}, bf16[2048,128]{1,0:T(8,128)(2,1)}, u32[]{:S(2)}) %copy-start.1) | copy-done | bytes 524312
  4.6 1.0 %copy-done.2 = bf16[2048,128]{1,0:T(8,128)(2,1)S(1)} copy-done((bf16[2048,128]{1,0:T(8,128)(2,1)S(1)}, bf16[2048,128]{1,0:T(8,128)(2,1)}, u32[]{:S(2)}) %copy-start.2) | copy-done | bytes 524312
  5.6 0.9 %copy-done.3 = bf16[256,4,128]{2,1,0:T(4,128)(2,1)S(1)} copy-done((bf16[256,4,128]{2,1,0:T(4,128)(2,1)S(1)}, bf16[256,4,128]{2,1,0:T(4,128)(2,1)}, u32[]{:S(2)}) %copy-start.3) | copy-done | bytes 262168
  6.6 0.8 %copy-done.4 = bf16[2048,1,16]{0,2,1:T(8,128)(2,1)S(1)} copy-done((bf16[2048,1,16]{0,2,1:T(8,128)(2,1)S(1)}, bf16[2048,1,16]{0,2,1:T(8,128)(2,1)}, u32[]{:S(2)}) %copy-start.4) | copy-done | bytes 65560
  7.4 0.8 %copy-done.5 = bf16[2048,1,16]{0,2,1:T(8,128)(2,1)S(1)} copy-done((bf16[2048,1,16]{0,2,1:T(8,128)(2,1)S(1)}, bf16[2048,1,16]{0,2,1:T(8,128)(2,1)}, u32[]{:S(2)}) %copy-start.5) | copy-done | bytes 65560
  8.3 0.8 %copy-done.6 = bf16[1,16,2048]{2,1,0:T(8,128)(2,1)S(1)} copy-done((bf16[1,16,2048]{2,1,0:T(8,128)(2,1)S(1)}, bf16[1,16,2048]{2,1,0:T(8,128)(2,1)}, u32[]{:S(2)}) %copy-start.6) | copy-done | bytes 65560
  9.1 0.8 copy-done.7
  9.9 0.8 copy-done.8
  10.6 0.7 copy-done.9
  11.3 0.7 copy-done.10
  12.0 0.7 copy-done.11
  12.7 0.7 copy-done.12
  13.4 0.7 copy-done.13
  14.1 0.7 copy-done.14
  14.8 0.7 copy-done.15
  15.5 0.7 copy-done.16
  16.1 0.7 copy-done.17
  16.8 62.7 %shard_map.203 = (bf16[4,16,256]{2,1,0:T(8,128)(2,1)S(1)}, f32[4096,128]{1,0:T(8,128)S(1)}) custom-call(bf16[4,16,256]{2,1,0:T(8,128)(2,1)S(1)} %bitcast.34, bf16[1,2048]{1,0:T(2,128)(2,1)S(1)} %reshape.37.gain_ref, bf16[2048,128]{1,0:T(8,128)(2,1)S(1)} %copy-done.1, bf16[2048,128]{1,0:T(8,128)(2,1)S(1)} %copy-done.2, bf16[16,2048]{1,0:T(8,128)(2,1)S(1)} %bitcast.31, ...), custom_call_target="tpu_custom_call" | custom-call | tf_op jit(solution)/shard_map/pallas_call | solution.py:382
  79.5 0.6 copy.27
  80.1 1.3 %copy.28 = f32[256,1,16,128]{3,2,1,0:T(8,128)} copy(f32[256,1,16,128]{3,2,1,0:T(8,128)S(1)} %bitcast.29) | data formatting | bytes 4194304
  (16 shorter events, 0.0 us)
Async XLA Ops:
  2.0 1.6 %copy-start = (f32[256,1,16,128]{3,2,1,0:T(8,128)S(1)}, f32[256,1,16,128]{3,2,1,0:T(8,128)}, u32[]{:S(2)}) copy-start(f32[256,1,16,128]{3,2,1,0:T(8,128)} %param.33) | copy-start | bytes 6291460
  3.6 1.0 %copy-start.1 = (bf16[2048,128]{1,0:T(8,128)(2,1)S(1)}, bf16[2048,128]{1,0:T(8,128)(2,1)}, u32[]{:S(2)}) copy-start(bf16[2048,128]{1,0:T(8,128)(2,1)} %wq_ref.1) | copy-start | bytes 1572868
  4.6 1.0 %copy-start.2 = (bf16[2048,128]{1,0:T(8,128)(2,1)S(1)}, bf16[2048,128]{1,0:T(8,128)(2,1)}, u32[]{:S(2)}) copy-start(bf16[2048,128]{1,0:T(8,128)(2,1)} %wk_ref.1) | copy-start | bytes 1572868
  5.6 0.9 %copy-start.3 = (bf16[256,4,128]{2,1,0:T(4,128)(2,1)S(1)}, bf16[256,4,128]{2,1,0:T(4,128)(2,1)}, u32[]{:S(2)}) copy-start(bf16[256,4,128]{2,1,0:T(4,128)(2,1)} %param.34) | copy-start | bytes 786436
  6.6 0.8 %copy-start.4 = (bf16[2048,1,16]{0,2,1:T(8,128)(2,1)S(1)}, bf16[2048,1,16]{0,2,1:T(8,128)(2,1)}, u32[]{:S(2)}) copy-start(bf16[2048,1,16]{0,2,1:T(8,128)(2,1)} %param.24) | copy-start | bytes 196612
  7.4 0.8 %copy-start.5 = (bf16[2048,1,16]{0,2,1:T(8,128)(2,1)S(1)}, bf16[2048,1,16]{0,2,1:T(8,128)(2,1)}, u32[]{:S(2)}) copy-start(bf16[2048,1,16]{0,2,1:T(8,128)(2,1)} %param.25) | copy-start | bytes 196612
  8.3 0.8 %copy-start.6 = (bf16[1,16,2048]{2,1,0:T(8,128)(2,1)S(1)}, bf16[1,16,2048]{2,1,0:T(8,128)(2,1)}, u32[]{:S(2)}) copy-start(bf16[1,16,2048]{2,1,0:T(8,128)(2,1)} %param.31) | copy-start | bytes 196612
  9.1 0.8 copy-start.7
  9.9 0.8 copy-start.8
  10.6 0.7 copy-start.9
  11.3 0.7 copy-start.10
  12.0 0.7 copy-start.11
  12.7 0.7 copy-start.12
  13.4 0.7 copy-start.13
  14.1 0.7 copy-start.14
  14.8 0.7 copy-start.15
  15.5 0.7 copy-start.16
  16.1 0.7 copy-start.17
where the time goes:
time: 82.2 us; the launch traced here: 81.4 us
  Pallas kernels  62.7 us (76%)
  local copies, waits for them, and re-layouts  17.4 us (21%)
  between operations  1.3 us (2%)
    pallas_call x1, Pallas kernels, on_device(): pl.pallas_call(functools.partial(kernel, tp_n, kv_n), out_shape=(jax.Shap...  62.7 us
    unnamed x38, local copies, waits for them, and re-layouts  16.7 us

commit v1 on v0

v1 whole, which is shorter than its diff:
```python
import functools

import jax
import jax.numpy as jnp
from jax import lax
from jax.experimental import pallas as pl
from jax.experimental.pallas import tpu as pltpu
from jax.sharding import PartitionSpec as P

EPS = 1e-06
INPUTS = 20
F32 = jnp.float32
BF16 = jnp.bfloat16
MESH = pl.DeviceIdType.MESH
NT = (((1,), (1,)), ((), ()))
NN = (((1,), (0,)), ((), ()))
TN = (((0,), (0,)), ((), ()))


def dot(a, b, dims=NN):
    return lax.dot_general(a, b, dims, preferred_element_type=F32)


def iota(shape, dim):
    return lax.broadcasted_iota(jnp.int32, shape, dim)


def roll(x, shift):
    return x if shift % 128 == 0 else pltpu.roll(x, shift % 128, 1)


def row_to_column(row):
    n = row.shape[1]
    square = jnp.broadcast_to(row, (n, n))
    return jnp.sum(jnp.where(iota((n, n), 0) == iota((n, n), 1), square, 0.0), axis=1, keepdims=True)


def ungroup(parts, j):
    chunk = iota(parts[0].shape, 1) // 32
    halves = []
    for h in range(2):
        total = None
        for m in range(4):
            x = roll(parts[h * 4 + m], (m - j) * 32)
            total = x if total is None else jnp.where(chunk == m, x, total)
        halves.append(total)
    return jnp.concatenate(halves, axis=1)


def regroup(rows, g):
    h, m = divmod(g, 4)
    total = None
    for j in range(4):
        x = roll(rows[j][:, h * 128 : h * 128 + 128], (j - m) * 32)
        total = x if total is None else jnp.where(iota(x.shape, 1) // 32 == j, x, total)
    return total


def pick_rows(product):
    lanes = product.shape[1]
    cube = product.reshape(32, 16, lanes)
    keep = iota(cube.shape, 0) == iota(cube.shape, 2) % 32
    return jnp.sum(jnp.where(keep, cube, 0.0), axis=0)


def pick_pairs(product):
    n, lanes = product.shape[0] // 32, product.shape[1]
    cube = product.reshape(n, 32, lanes)
    keep = iota(cube.shape, 1) == iota(cube.shape, 2) % 32
    return jnp.sum(jnp.where(keep, cube, 0.0), axis=1)


def sum_of(terms):
    return functools.reduce(lambda a, b: a + b, terms)


def old_part(state, keys, old_values, log_decay, strengths, accepted, store):
    source, target = iota((128, 128), 1), iota((128, 128), 0)
    order = (source == (target % 32) * 4 + target // 32).astype(BF16)
    grouped, reads, grams = [], [], []
    for g in range(8):
        kg = dot(order, keys(g)).astype(BF16)
        grouped.append(kg)
        reads.append(pick_rows(dot(state(g).astype(BF16), kg, NT)))
        grams.append(pick_pairs(dot(kg, kg, NT)))
    gram = [ungroup(grams, j) for j in range(4)]
    read = [ungroup(reads, j) for j in range(4)]
    inv = [lax.rsqrt(gram[j][j : j + 1] + EPS) for j in range(4)]
    gam, beta = [], []
    for j in range(4):
        live = (j < accepted).astype(F32)
        g_j = log_decay[j] * live
        gam.append(g_j if j == 0 else gam[-1] + g_j)
        beta.append(strengths[j] * live)
    update = []
    for i in range(4):
        u = beta[i] * (old_values[i] - (jnp.exp(gam[i]) * inv[i]) * read[i])
        for j in range(i):
            a = beta[i] * (gram[j][i : i + 1] * (inv[i] * inv[j])) * jnp.exp(gam[i] - gam[j])
            u = u - a * update[j]
        update.append(u)
    weighted = [update[j] * (jnp.exp(gam[3] - gam[j]) * inv[j]) for j in range(4)]
    kept = jnp.exp(gam[3])
    columns = [jnp.broadcast_to(row_to_column(kept[:, h * 128 : h * 128 + 128]), (128, 128)) for h in range(2)]
    for g in range(8):
        wg = regroup(weighted, g)
        cube = (32, 16, 128)
        keep = iota(cube, 0) == iota(cube, 2) % 32
        block = jnp.where(keep, jnp.broadcast_to(wg[None], cube), 0.0).reshape(512, 128).astype(BF16)
        h, m = divmod(g, 4)
        scale = jnp.broadcast_to(columns[h][m * 32 : m * 32 + 32][:, None, :], cube).reshape(512, 128)
        store(g, scale * state(g) + dot(block, grouped[g]))


def new_part(accepted_state, query_key, values, beta_pre, decay_pre, rate, proposal, parent):
    reads, grams = [], []
    for g in range(8):
        qk = query_key(g)
        reads.append(pick_rows(dot(accepted_state(g), qk, NT)))
        grams.append(pick_pairs(dot(qk, qk, NT)))
    left = [r[:, :128] for r in reads], [r[:, 128:] for r in reads]
    aq = [ungroup(left[0], j) for j in range(4)]
    ak = [ungroup(left[1], j) for j in range(4)]
    gq = [ungroup([r[:, :128] for r in grams], j) for j in range(4)]
    gk = [ungroup([r[:, 128:] for r in grams], j) for j in range(4)]
    inv_q = [lax.rsqrt(gq[j][j : j + 1] + EPS) * (128.0**-0.5) for j in range(4)]
    inv_k = [lax.rsqrt(gk[j][4 + j : 5 + j] + EPS) for j in range(4)]
    ancestors = []
    for i in range(4):
        row = {j: (parent[i] == j).astype(F32) for j in range(i)}
        row = {j: row[j] + sum_of([jnp.zeros_like(row[j])] + [row[m] * ancestors[m][j] for m in range(j + 1, i)]) for j in range(i)}
        ancestors.append(row)
    beta, g_new, gam = [], [], []
    for i in range(4):
        x = decay_pre[i]
        softplus = jnp.maximum(x, 0.0) + jnp.log1p(jnp.exp(-jnp.abs(x)))
        g_new.append(-rate * softplus + proposal[i])
        beta.append(jax.nn.sigmoid(beta_pre[i]))
        gam.append(sum_of([g_new[i]] + [ancestors[i][j] * g_new[j] for j in range(i)]))
    outputs, update = [], []
    for i in range(4):
        grow = jnp.exp(gam[i])
        u = beta[i] * (values[i] - (grow * inv_k[i]) * ak[i])
        o = (grow * inv_q[i]) * aq[i]
        for j in range(i):
            reach = jnp.exp(jnp.minimum(gam[i] - gam[j], 0.0)) * ancestors[i][j] * inv_k[j]
            u = u - (beta[i] * inv_k[i] * gk[j][4 + i : 5 + i] * reach) * update[j]
            o = o + (inv_q[i] * gk[j][i : i + 1] * reach) * update[j]
        update.append(u)
        o = o + (inv_q[i] * gk[i][i : i + 1] * inv_k[i]) * u
        outputs.append(o)
    return outputs


def kernel(
    tp_n, kv_n, *refs,
):
    sources, (out_ref, acc_ref), held, scratch = refs[:INPUTS], refs[INPUTS : INPUTS + 2], refs[INPUTS + 2 : 2 * INPUTS + 2], refs[2 * INPUTS + 2 :]
    run(tp_n, kv_n, sources, out_ref, acc_ref, *held, *scratch)


def run(
    tp_n, kv_n, sources, out_ref, acc_ref,
    xt_ref, wv_ref, wz_ref, wo_ref, gain_ref, keys_ref, state_ref, oldv_ref, logd_ref, strength_ref, accepted_ref,
    wq_ref, wk_ref, ws_ref, wd_ref, rate_ref, prop_ref, parent_ref, hgain_ref, ogain_ref,
    load_sems, accv, acc_sems,
    xall, wvz, woall, gaincol, xnorm, qkall, vzs, vzall, sdall, abf, ybuf, yall, sqs, sqall, csend, call, sqf,
    st, rt, sv, rv, swm, rwm, sq, rq, ssd, rsd, sqm, rqm, sdm, rdm, svz, rvz, so, ro, som, rom, se, re, ses, res, sf, rf, sh, rh,
):
    held = (
        xt_ref, wv_ref, wz_ref, wo_ref, gain_ref, keys_ref, state_ref, oldv_ref, logd_ref, strength_ref, accepted_ref,
        wq_ref, wk_ref, ws_ref, wd_ref, rate_ref, prop_ref, parent_ref, hgain_ref, ogain_ref,
    )
    loads = [pltpu.make_async_copy(src, dst, load_sems.at[n]) for n, (src, dst) in enumerate(zip(sources, held))]
    for c in loads:
        c.start()
    kv, tp = lax.axis_index("kv"), lax.axis_index("tp")
    chip, core = tp // 2, lax.rem(tp, 2)
    mate = tp + 1 - 2 * core
    own = kv * tp_n + tp
    everyone = [(a, b) for a in range(kv_n) for b in range(tp_n) if a or b]

    def device(a, b):
        return lax.rem(kv + a, kv_n), lax.rem(tp + b, tp_n)

    def send(src, dst, send_sem, recv_sem, target):
        c = remote(src, dst, send_sem, recv_sem, target)
        c.start()
        return c

    def remote(src, dst, send_sem, recv_sem, target):
        return pltpu.make_async_remote_copy(
            src_ref=src, dst_ref=dst, send_sem=send_sem, recv_sem=recv_sem, device_id=target, device_id_type=MESH
        )

    def total(ref, send_sem, recv_sem):
        return remote(ref, ref, send_sem, recv_sem, (kv, mate))

    def along_chips(d):
        return lax.rem(chip + d, 4) * 2 + core

    def lanes_of(t):
        return pl.ds(pl.multiple_of(lax.rem(t, 2) * 128, 128), 128)

    barrier = pltpu.get_barrier_semaphore()
    for a, b in everyone:
        pl.semaphore_signal(barrier, inc=1, device_id=device(a, b), device_id_type=MESH)
    for c in loads[:5]:
        c.wait()
    with jax.named_scope("barrier"):
        pl.semaphore_wait(barrier, kv_n * tp_n - 1)

    with jax.named_scope("issue_t"):
        own_rows = pl.ds(pl.multiple_of(own * 16, 16), 16)
        for a, b in everyone:
            k, t = device(a, b)
            send(xt_ref.at[t // 2, :, lanes_of(t)], xall.at[own_rows], st, rt, (k, t))
        xall[own_rows, :] = xt_ref[tp // 2, :, lanes_of(tp)]
        tokens = total(xall.at[0:2032], st, rt)

    stage_w = []
    for d in range(1, 4):
        stage_w.append(send(wv_ref, wvz.at[core, chip, 0], sv.at[d], rv.at[d], (kv, along_chips(d))))
        stage_w.append(send(wz_ref, wvz.at[core, chip, 1], sv.at[4 + d], rv.at[4 + d], (kv, along_chips(d))))
    wvz[core, chip, 0] = wv_ref[...]
    wvz[core, chip, 1] = wz_ref[...]
    for n in range(16):
        column = row_to_column(gain_ref[n : n + 1, :].astype(F32))
        gaincol[n * 128 : n * 128 + 128, :] = jnp.broadcast_to(column, (128, 128))
    for c in loads[5:]:
        c.wait()

    saves = []

    def store(g, value):
        rows = slice(g * 512, g * 512 + 512)
        accv[rows, :] = value
        saves.append(pltpu.make_async_copy(accv.at[rows], acc_ref.at[rows], acc_sems.at[g]))
        saves[-1].start()
        abf[g * 512 : g * 512 + 512, :] = value.astype(BF16)

    with jax.named_scope("old"):
        old_part(
            lambda g: state_ref[g * 512 : g * 512 + 512, :],
            lambda g: keys_ref[g * 128 : g * 128 + 128, :],
            [oldv_ref[j].astype(F32) for j in range(4)],
            [logd_ref[j] for j in range(4)],
            [strength_ref[j] for j in range(4)],
            accepted_ref[...],
            store,
        )

    with jax.named_scope("wait_t"):
        tokens.wait_recv()
    with jax.named_scope("project"):
        squares = sum_of([jnp.sum(jnp.square(xall[n * 128 : n * 128 + 128, :].astype(F32)), axis=0, keepdims=True) for n in range(16)])
        scale = lax.rsqrt(squares / 2048.0 + EPS)
        for n in range(16):
            rows = slice(n * 128, n * 128 + 128)
            xnorm[rows, :] = (xall[rows, :].astype(F32) * scale * gaincol[rows, :]).astype(BF16)
        x = xnorm[...]
        qkall[tp, :, 0:128] = dot(x, wq_ref[...], TN).astype(BF16)
        qkall[tp, :, 128:256] = dot(x, wk_ref[...], TN).astype(BF16)
        first = iota((16, 2048), 0) == 0
        wsd = jnp.where(first, jnp.broadcast_to(ws_ref[...].astype(F32), (16, 2048)), jnp.broadcast_to(wd_ref[...].astype(F32), (16, 2048)))
        sdall[tp] = dot(wsd.astype(BF16), x)[0:8]
    stage_c = []
    for d in range(1, 4):
        target = (kv, along_chips(d))
        stage_c.append((send(qkall.at[tp], qkall.at[tp], sq.at[d], rq.at[d], target), send(sdall.at[tp], sdall.at[tp], ssd.at[d], rsd.at[d], target)))
    stage_m = [send(qkall.at[tp], qkall.at[tp], sqm.at[0], rqm.at[0], (kv, mate)), send(sdall.at[tp], sdall.at[tp], sdm.at[0], rdm.at[0], (kv, mate))]
    with jax.named_scope("wait_w"):
        for c in stage_w:
            c.wait_recv()
    to_mate = send(wvz.at[core], wvz.at[core], swm, rwm, (kv, mate))
    with jax.named_scope("wait_wm"):
        to_mate.wait_recv()
    vzs[...] = dot(wvz[...].reshape(256, 2048), xnorm[...]).astype(BF16).reshape(8, 2, 16, 128)
    stage_v = []
    for b in range(1, tp_n):
        _, t = device(0, b)
        stage_v.append(send(vzs.at[lax.rem(t, 2) * 4 + t // 2], vzall.at[tp], svz.at[b], rvz.at[b], (kv, t)))
    vzall[tp] = vzs[core * 4 + chip]
    with jax.named_scope("wait_c"):
        for d in range(1, 4):
            for c in stage_c[d - 1]:
                c.wait_recv()
            source = lax.rem(chip + 4 - d, 4) * 2 + core
            stage_m.append(send(qkall.at[source], qkall.at[source], sqm.at[d], rqm.at[d], (kv, mate)))
            stage_m.append(send(sdall.at[source], sdall.at[source], sdm.at[d], rdm.at[d], (kv, mate)))
    for a in range(kv_n):
        k = lax.rem(kv + a, kv_n)
        for d in range(4):
            if a or d:
                cols = pl.ds(pl.multiple_of(k * 128, 128), 128)
                send(wo_ref.at[:, cols], woall.at[core, kv, chip], so, ro, (k, along_chips(d)))
    woall[core, kv, chip] = wo_ref[:, pl.ds(pl.multiple_of(kv * 128, 128), 128)]
    with jax.named_scope("wait_m"):
        for c in stage_m + stage_v:
            c.wait_recv()

    def query_key(g):
        h, m = divmod(g, 4)
        pieces = [qkall[p * 2 + h, m * 32 : m * 32 + 32, s * 128 : s * 128 + 128] for s in range(2) for p in range(4)]
        return jnp.concatenate(pieces, axis=0)

    def both(f):
        return [jnp.concatenate([f(p * 2), f(p * 2 + 1)], axis=1) for p in range(4)]

    with jax.named_scope("new"):
        outputs = new_part(
            lambda g: abf[g * 512 : g * 512 + 512, :],
            query_key,
            both(lambda t: vzall[t, 0].astype(F32)),
            both(lambda t: sdall[t, 0:1, :]),
            both(lambda t: sdall[t, 1:2, :]),
            rate_ref[...],
            [prop_ref[j] for j in range(4)],
            [parent_ref[j : j + 1, :] for j in range(4)],
        )
        zgate = both(lambda t: vzall[t, 1].astype(F32))
        hgain = jnp.broadcast_to(row_to_column(hgain_ref[...].astype(F32)), (16, 256))
        for t in range(8):
            half = slice((t % 2) * 128, (t % 2) * 128 + 128)
            o, z = outputs[t // 2][:, half], zgate[t // 2][:, half]
            sqs[t] = jnp.sum(jnp.square(o), axis=0, keepdims=True)
            ybuf[t] = (o * hgain[:, half] * (z * jax.nn.sigmoid(z))).astype(BF16)
    with jax.named_scope("issue_e"):
        for a, b in everyone:
            k, t = device(a, b)
            send(sqs.at[t], sqall.at[own], ses, res, (k, t))
            send(ybuf.at[t], yall.at[core, kv, chip], se, re, (k, t))
        sqall[own] = sqs[tp]
        yall[core, kv, chip] = ybuf[tp]
    with jax.named_scope("wait_o"):
        out_weights = total(xall.at[0:1008], so, ro)
        out_weights.wait_recv()
    out_mate = send(woall.at[core], woall.at[core], som, rom, (kv, mate))
    with jax.named_scope("wait_om"):
        out_mate.wait_recv()
    with jax.named_scope("wait_e"):
        all_y, all_sq = total(xall.at[0:2032], se, re), total(sqall.at[0:127], ses, res)
        all_sq.wait_recv()
        all_y.wait_recv()
    with jax.named_scope("combine"):
        for k in range(16):
            scale = lax.rsqrt(sum_of([sqall[k * 8 + t] for t in range(8)]) / 128.0 + EPS)
            for c in range(2):
                for n in range(4):
                    rows = slice(((c * 16 + k) * 4 + n) * 16, ((c * 16 + k) * 4 + n) * 16 + 16)
                    xnorm[rows, :] = (yall[c, k, n].astype(F32) * scale).astype(BF16)
        combined = dot(woall[...].reshape(2048, 128), xnorm[...], TN)
        csend[...] = combined.reshape(8, 16, 128)
        sqf[tp * 16 + kv] = jnp.sum(jnp.square(combined), axis=0, keepdims=True)
    slot = sqf.at[tp * 16 + kv]
    for a, b in everyone:
        send(slot, slot, sh, rh, device(a, b))
    stage_f = []
    for b in range(1, tp_n):
        _, t = device(0, b)
        stage_f.append(send(csend.at[t], call.at[tp], sf.at[b], rf.at[b], (kv, t)))
    call[tp] = csend[tp]
    ogain = jnp.broadcast_to(row_to_column(ogain_ref[...].astype(F32)), (16, 128))
    sums = total(sqf.at[0:127], sh, rh)
    with jax.named_scope("sends"):
        for pair in stage_c:
            for c in pair:
                c.wait_send()
        for c in stage_w + stage_m + stage_v + [tokens, to_mate, out_weights, out_mate, all_y, all_sq]:
            c.wait_send()
    with jax.named_scope("wait_f"):
        for c in stage_f:
            c.wait_recv()
    with jax.named_scope("wait_h"):
        sums.wait_recv()
    for t in range(8):
        scale = lax.rsqrt(sum_of([sqf[t * 16 + k] for k in range(16)]) / 2048.0 + EPS)
        out_ref[t // 2, :, (t % 2) * 128 : (t % 2) * 128 + 128] = (call[t] * scale * ogain).astype(BF16)
    for c in stage_f + [sums]:
        c.wait_send()
    for c in saves:
        c.wait()


def hand_over(out_in, acc_in, out_ref, acc_ref, outv, accv, loaded, saved):
    pieces = [(out_in, outv, out_ref)]
    for g in range(8):
        rows = pl.ds(g * 512, 512)
        pieces.append((acc_in.at[rows], accv.at[rows], acc_ref.at[rows]))
    loads = [pltpu.make_async_copy(a, b, loaded.at[n]) for n, (a, b, _) in enumerate(pieces)]
    saves = [pltpu.make_async_copy(b, c, saved.at[n]) for n, (_, b, c) in enumerate(pieces)]
    for c in loads:
        c.start()
    for load, save in zip(loads, saves):
        load.wait()
        save.start()
    for c in saves:
        c.wait()


def on_device(
    tokens, input_norm_gain, query_weight, key_weight, value_weight, output_gate_weight, strength_weight, decay_weight,
    head_decay_rate, proposal_log_decay, head_norm_gain, output_weight, output_norm_gain, state, previous_keys,
    previous_values, previous_log_decay, previous_strengths, accepted, parent,
):
    tp_n, kv_n = lax.axis_size("tp"), lax.axis_size("kv")
    args = [
        tokens.transpose(1, 2, 0),
        value_weight.transpose(1, 2, 0).reshape(16, 2048),
        output_gate_weight.transpose(1, 2, 0).reshape(16, 2048),
        output_weight.reshape(16, 2048),
        input_norm_gain.reshape(16, 128),
        previous_keys.reshape(1024, 128),
        state.reshape(4096, 128),
        previous_values.transpose(1, 2, 3, 0).reshape(4, 16, 256),
        previous_log_decay.transpose(1, 2, 0),
        previous_strengths.transpose(1, 2, 0),
        accepted.reshape(1, 256),
        query_weight,
        key_weight,
        strength_weight.transpose(1, 0),
        decay_weight.transpose(1, 0),
        head_decay_rate.reshape(1, 1),
        proposal_log_decay.transpose(1, 2, 0),
        parent.transpose(1, 0),
        head_norm_gain.reshape(1, 16),
        output_norm_gain.reshape(1, 16),
    ]
    vmem = pl.BlockSpec(memory_space=pltpu.VMEM)
    hbm = pl.BlockSpec(memory_space=pltpu.HBM)
    specs = [hbm] * len(args)

    def sems(n):
        return [pltpu.SemaphoreType.DMA((n,)), pltpu.SemaphoreType.DMA((n,))]

    def one():
        return [pltpu.SemaphoreType.DMA(()), pltpu.SemaphoreType.DMA(())]

    out, acc = pl.pallas_call(
        functools.partial(kernel, tp_n, kv_n),
        out_shape=(jax.ShapeDtypeStruct((4, 16, 256), BF16), jax.ShapeDtypeStruct((4096, 128), F32)),
        in_specs=specs,
        out_specs=(vmem, hbm),
        scratch_shapes=[
            *[pltpu.VMEM(a.shape, a.dtype) for a in args],
            pltpu.SemaphoreType.DMA((len(args),)),
            pltpu.VMEM((4096, 128), F32),
            pltpu.SemaphoreType.DMA((8,)),
            pltpu.VMEM((2048, 128), BF16),
            pltpu.VMEM((2, 4, 2, 16, 2048), BF16),
            pltpu.VMEM((2, 16, 4, 16, 128), BF16),
            pltpu.VMEM((2048, 128), F32),
            pltpu.VMEM((2048, 128), BF16),
            pltpu.VMEM((8, 128, 256), BF16),
            pltpu.VMEM((8, 2, 16, 128), BF16),
            pltpu.VMEM((8, 2, 16, 128), BF16),
            pltpu.VMEM((8, 8, 128), F32),
            pltpu.VMEM((4096, 128), BF16),
            pltpu.VMEM((8, 16, 128), BF16),
            pltpu.VMEM((2, 16, 4, 16, 128), BF16),
            pltpu.VMEM((8, 1, 128), F32),
            pltpu.VMEM((128, 1, 128), F32),
            pltpu.VMEM((8, 16, 128), F32),
            pltpu.VMEM((8, 16, 128), F32),
            pltpu.VMEM((128, 1, 128), F32),
            *one(), *sems(8), *one(), *sems(4), *sems(4), *sems(4), *sems(4), *sems(8), *one(), *one(), *one(), *one(), *sems(8), *one(),
        ],
        compiler_params=pltpu.CompilerParams(collective_id=0, has_side_effects=True, vmem_limit_bytes=67043328),
    )(*args)
    out, acc = pl.pallas_call(
        hand_over,
        out_shape=(jax.ShapeDtypeStruct((4, 16, 256), BF16), jax.ShapeDtypeStruct((4096, 128), F32)),
        in_specs=(hbm, hbm),
        out_specs=(hbm, hbm),
        scratch_shapes=[pltpu.VMEM((4, 16, 256), BF16), pltpu.VMEM((4096, 128), F32), *sems(9)],
        compiler_params=pltpu.CompilerParams(vmem_limit_bytes=67043328),
    )(out, acc)
    return out.transpose(2, 0, 1), acc.reshape(256, 1, 16, 128)


def solution(mesh):
    placed = (
        P(None, None, ("kv", "tp")),
        P(),
        P(None, "kv"),
        P(None, "kv"),
        P(None, "kv", "tp"),
        P(None, "kv", "tp"),
        P(None, "kv"),
        P(None, "kv"),
        P("kv"),
        P(None, None, "kv"),
        P("tp"),
        P("kv", "tp", None),
        P(("kv", "tp")),
        P(None, "kv", "tp", None),
        P(None, None, "kv"),
        P(None, None, "kv", "tp"),
        P(None, None, "kv"),
        P(None, None, "kv"),
        P(),
        P(),
    )
    return jax.shard_map(
        on_device,
        mesh=mesh,
        in_specs=placed,
        out_specs=(P(None, None, ("kv", "tp")), P(None, "kv", "tp", None)),
        check_vma=False,
    )
```

time: 82.2 us -> 54.7 us (0.67)
  local copies, waits for them, and re-layouts: 17.4 us -> 0 us
  Pallas kernels: 62.7 us -> 53.3 us
    unnamed x38 -> x0, local copies, waits for them, and re-layouts: 16.7 us -> none
    pallas_call x1, Pallas kernels: 62.7 us -> 50.8 us  [on_device(): pl.pallas_call(functools.partial(kernel, tp_n, kv_n), out_shape=(jax.Shap...]
    pallas_call x0 -> x1, Pallas kernels: none -> 2.43 us  [on_device(): pl.pallas_call(hand_over, out_shape=(jax.ShapeDtypeStruct((4, 16, 256), B...]
where the time goes in v1:
time: 54.7 us; the launch traced here: 54.6 us
  Pallas kernels  53.3 us (97%)
  between operations  1.29 us (2%)
    pallas_call x1, Pallas kernels, on_device(): pl.pallas_call(functools.partial(kernel, tp_n, kv_n), out_shape=(jax.Shap...  50.8 us
    pallas_call x1, Pallas kernels, on_device(): pl.pallas_call(hand_over, out_shape=(jax.ShapeDtypeStruct((4, 16, 256), B...  2.43 us

profile of v1, /device:TPU:1, one launch (start us, length us, event | category | flops | bytes accessed | tf_op | source)
XLA Modules:
  0.0 54.6 jit_solution(15344179254179236473)
XLA Ops:
  1.3 50.8 %shard_map.203 = (bf16[4,16,256]{2,1,0:T(8,128)(2,1)}, f32[4096,128]{1,0:T(8,128)}) custom-call(bf16[4,16,256]{2,1,0:T(8,128)(2,1)} %bitcast.36, bf16[16,2048]{1,0:T(8,128)(2,1)} %bitcast.33, bf16[16,2048]{1,0:T(8,128)(2,1)} %bitcast.34, bf16[16,2048]{1,0:T(8,128)(2,1)} %bitcast.35, bf16[16,128]{1,0:T(8,128)(2,1)} %bitcast.40, bf16[1024,128]{1,0:T(8,128)(2,1)} %bitcast.32, ...), custom_call_target="tpu_custom_call" | custom-call | tf_op jit(solution)/shard_map/pallas_call | solution.py:439
  52.1 2.4 %shard_map.204 = (bf16[4,16,256]{2,1,0:T(8,128)(2,1)}, f32[4096,128]{1,0:T(8,128)}) custom-call(bf16[4,16,256]{2,1,0:T(8,128)(2,1)} %get-tuple-element.6.out_in, f32[4096,128]{1,0:T(8,128)} %get-tuple-element.7.acc_in), custom_call_target="tpu_custom_call" | custom-call | tf_op jit(solution)/shard_map/pallas_call | solution.py:470

commit v2 on v1

--- a/solution.py
+++ b/solution.py
@@ -1,4 +1,5 @@
 import functools
+import itertools
 
 import jax
 import jax.numpy as jnp
@@ -8,7 +9,7 @@
 from jax.sharding import PartitionSpec as P
 
 EPS = 1e-06
-INPUTS = 20
+INPUTS = 19
 F32 = jnp.float32
 BF16 = jnp.bfloat16
 MESH = pl.DeviceIdType.MESH
@@ -72,6 +73,10 @@
 
 def sum_of(terms):
     return functools.reduce(lambda a, b: a + b, terms)
+
+
+def far_first(offsets):
+    return sorted([o for o in offsets if any(o)], key=lambda o: -sum(min(d, 4 - d) for d in o[:3]))
 
 
 def old_part(state, keys, old_values, log_decay, strengths, accepted, store):
@@ -155,33 +160,32 @@
 def kernel(
     tp_n, kv_n, *refs,
 ):
-    sources, (out_ref, acc_ref), held, scratch = refs[:INPUTS], refs[INPUTS : INPUTS + 2], refs[INPUTS + 2 : 2 * INPUTS + 2], refs[2 * INPUTS + 2 :]
-    run(tp_n, kv_n, sources, out_ref, acc_ref, *held, *scratch)
+    run(tp_n, kv_n, refs[:INPUTS], *refs[INPUTS:])
 
 
 def run(
-    tp_n, kv_n, sources, out_ref, acc_ref,
+    tp_n, kv_n, sources, sums_ref, comb_ref, acc_ref,
     xt_ref, wv_ref, wz_ref, wo_ref, gain_ref, keys_ref, state_ref, oldv_ref, logd_ref, strength_ref, accepted_ref,
-    wq_ref, wk_ref, ws_ref, wd_ref, rate_ref, prop_ref, parent_ref, hgain_ref, ogain_ref,
+    wq_ref, wk_ref, ws_ref, wd_ref, rate_ref, prop_ref, parent_ref, hgain_ref,
     load_sems, accv, acc_sems,
-    xall, wvz, woall, gaincol, xnorm, qkall, vzs, vzall, sdall, abf, ybuf, yall, sqs, sqall, csend, call, sqf,
+    xall, wvz, woall, gaincol, xnorm, qkall, vzs, vzall, sdall, abf, ybuf, yall, sqs, sqall, csend, sqf,
     st, rt, sv, rv, swm, rwm, sq, rq, ssd, rsd, sqm, rqm, sdm, rdm, svz, rvz, so, ro, som, rom, se, re, ses, res, sf, rf, sh, rh,
 ):
     held = (
         xt_ref, wv_ref, wz_ref, wo_ref, gain_ref, keys_ref, state_ref, oldv_ref, logd_ref, strength_ref, accepted_ref,
-        wq_ref, wk_ref, ws_ref, wd_ref, rate_ref, prop_ref, parent_ref, hgain_ref, ogain_ref,
+        wq_ref, wk_ref, ws_ref, wd_ref, rate_ref, prop_ref, parent_ref, hgain_ref,
     )
     loads = [pltpu.make_async_copy(src, dst, load_sems.at[n]) for n, (src, dst) in enumerate(zip(sources, held))]
-    for c in loads:
-        c.start()
     kv, tp = lax.axis_index("kv"), lax.axis_index("tp")
     chip, core = tp // 2, lax.rem(tp, 2)
     mate = tp + 1 - 2 * core
     own = kv * tp_n + tp
-    everyone = [(a, b) for a in range(kv_n) for b in range(tp_n) if a or b]
-
-    def device(a, b):
-        return lax.rem(kv + a, kv_n), lax.rem(tp + b, tp_n)
+    everyone = far_first(itertools.product(range(4), range(4), range(4), range(2)))
+    high, low = kv // 4, lax.rem(kv, 4)
+
+    def device(offset):
+        z, y, x, c = offset
+        return lax.rem(high + z, 4) * 4 + lax.rem(low + y, 4), lax.rem(chip + x, 4) * 2 + lax.rem(core + c, 2)
 
     def send(src, dst, send_sem, recv_sem, target):
         c = remote(src, dst, send_sem, recv_sem, target)
@@ -203,8 +207,12 @@
         return pl.ds(pl.multiple_of(lax.rem(t, 2) * 128, 128), 128)
 
     barrier = pltpu.get_barrier_semaphore()
-    for a, b in everyone:
-        pl.semaphore_signal(barrier, inc=1, device_id=device(a, b), device_id_type=MESH)
+    for c in loads[:5]:
+        c.start()
+    for o in everyone:
+        pl.semaphore_signal(barrier, inc=1, device_id=device(o), device_id_type=MESH)
+    for c in loads[5:]:
+        c.start()
     for c in loads[:5]:
         c.wait()
     with jax.named_scope("barrier"):
@@ -212,16 +220,29 @@
 
     with jax.named_scope("issue_t"):
         own_rows = pl.ds(pl.multiple_of(own * 16, 16), 16)
-        for a, b in everyone:
-            k, t = device(a, b)
+        for o in everyone:
+            k, t = device(o)
             send(xt_ref.at[t // 2, :, lanes_of(t)], xall.at[own_rows], st, rt, (k, t))
         xall[own_rows, :] = xt_ref[tp // 2, :, lanes_of(tp)]
         tokens = total(xall.at[0:2032], st, rt)
 
-    stage_w = []
-    for d in range(1, 4):
-        stage_w.append(send(wv_ref, wvz.at[core, chip, 0], sv.at[d], rv.at[d], (kv, along_chips(d))))
-        stage_w.append(send(wz_ref, wvz.at[core, chip, 1], sv.at[4 + d], rv.at[4 + d], (kv, along_chips(d))))
+    for o in far_first(itertools.product(range(4), range(4), [0], [0])):
+        k, _ = device(o)
+        cols = pl.ds(pl.multiple_of(k * 128, 128), 128)
+        send(wo_ref.at[:, cols], woall.at[core, chip, kv], so, ro, (k, tp))
+    woall[core, chip, kv] = wo_ref[:, pl.ds(pl.multiple_of(kv * 128, 128), 128)]
+
+    stage_w, stage_wm = [], []
+    for d in (2, 1, 3):
+        target = (kv, along_chips(d))
+        stage_w.append(
+            [
+                send(wv_ref, wvz.at[core, chip, 0], sv.at[d], rv.at[d], target),
+                send(wz_ref, wvz.at[core, chip, 1], sv.at[4 + d], rv.at[4 + d], target),
+            ]
+        )
+    stage_wm.append(send(wv_ref, wvz.at[core, chip, 0], swm.at[0], rwm.at[0], (kv, mate)))
+    stage_wm.append(send(wz_ref, wvz.at[core, chip, 1], swm.at[4], rwm.at[4], (kv, mate)))
     wvz[core, chip, 0] = wv_ref[...]
     wvz[core, chip, 1] = wz_ref[...]
     for n in range(16):
@@ -265,36 +286,38 @@
         wsd = jnp.where(first, jnp.broadcast_to(ws_ref[...].astype(F32), (16, 2048)), jnp.broadcast_to(wd_ref[...].astype(F32), (16, 2048)))
         sdall[tp] = dot(wsd.astype(BF16), x)[0:8]
     stage_c = []
-    for d in range(1, 4):
+    for d in (2, 1, 3):
         target = (kv, along_chips(d))
         stage_c.append((send(qkall.at[tp], qkall.at[tp], sq.at[d], rq.at[d], target), send(sdall.at[tp], sdall.at[tp], ssd.at[d], rsd.at[d], target)))
     stage_m = [send(qkall.at[tp], qkall.at[tp], sqm.at[0], rqm.at[0], (kv, mate)), send(sdall.at[tp], sdall.at[tp], sdm.at[0], rdm.at[0], (kv, mate))]
     with jax.named_scope("wait_w"):
-        for c in stage_w:
+        for d, pair in ((1, stage_w[1]), (3, stage_w[2]), (2, stage_w[0])):
+            for c in pair:
+                c.wait_recv()
+            block = wvz.at[core, lax.rem(chip + 4 - d, 4)]
+            stage_wm.append(send(block, block, swm.at[d], rwm.at[d], (kv, mate)))
+    with jax.named_scope("wait_wm"):
+        for c in stage_wm:
             c.wait_recv()
-    to_mate = send(wvz.at[core], wvz.at[core], swm, rwm, (kv, mate))
-    with jax.named_scope("wait_wm"):
-        to_mate.wait_recv()
     vzs[...] = dot(wvz[...].reshape(256, 2048), xnorm[...]).astype(BF16).reshape(8, 2, 16, 128)
     stage_v = []
-    for b in range(1, tp_n):
-        _, t = device(0, b)
+    along_tp = far_first(itertools.product([0], [0], range(4), range(2)))
+    for b, o in enumerate(along_tp):
+        _, t = device(o)
         stage_v.append(send(vzs.at[lax.rem(t, 2) * 4 + t // 2], vzall.at[tp], svz.at[b], rvz.at[b], (kv, t)))
     vzall[tp] = vzs[core * 4 + chip]
     with jax.named_scope("wait_c"):
-        for d in range(1, 4):
-            for c in stage_c[d - 1]:
+        for d, pair in ((1, stage_c[1]), (3, stage_c[2]), (2, stage_c[0])):
+            for c in pair:
                 c.wait_recv()
             source = lax.rem(chip + 4 - d, 4) * 2 + core
             stage_m.append(send(qkall.at[source], qkall.at[source], sqm.at[d], rqm.at[d], (kv, mate)))
             stage_m.append(send(sdall.at[source], sdall.at[source], sdm.at[d], rdm.at[d], (kv, mate)))
-    for a in range(kv_n):
-        k = lax.rem(kv + a, kv_n)
-        for d in range(4):
-            if a or d:
-                cols = pl.ds(pl.multiple_of(k * 128, 128), 128)
-                send(wo_ref.at[:, cols], woall.at[core, kv, chip], so, ro, (k, along_chips(d)))
-    woall[core, kv, chip] = wo_ref[:, pl.ds(pl.multiple_of(kv * 128, 128), 128)]
+    out_tiles = total(xall.at[0:240], so, ro)
+    out_tiles.wait_recv()
+    block = woall.at[core, chip]
+    stage_o = [send(block, block, som.at[d], rom.at[d], (kv, along_chips(d))) for d in (2, 1, 3)]
+    stage_o.append(send(block, block, som.at[0], rom.at[0], (kv, mate)))
     with jax.named_scope("wait_m"):
         for c in stage_m + stage_v:
             c.wait_recv()
@@ -326,18 +349,19 @@
             sqs[t] = jnp.sum(jnp.square(o), axis=0, keepdims=True)
             ybuf[t] = (o * hgain[:, half] * (z * jax.nn.sigmoid(z))).astype(BF16)
     with jax.named_scope("issue_e"):
-        for a, b in everyone:
-            k, t = device(a, b)
+        for o in everyone:
+            k, t = device(o)
             send(sqs.at[t], sqall.at[own], ses, res, (k, t))
-            send(ybuf.at[t], yall.at[core, kv, chip], se, re, (k, t))
+            send(ybuf.at[t], yall.at[core, chip, kv], se, re, (k, t))
         sqall[own] = sqs[tp]
-        yall[core, kv, chip] = ybuf[tp]
+        yall[core, chip, kv] = ybuf[tp]
     with jax.named_scope("wait_o"):
-        out_weights = total(xall.at[0:1008], so, ro)
-        out_weights.wait_recv()
-    out_mate = send(woall.at[core], woall.at[core], som, rom, (kv, mate))
-    with jax.named_scope("wait_om"):
-        out_mate.wait_recv()
+        for d, c in ((1, stage_o[1]), (3, stage_o[2]), (2, stage_o[0])):
+            c.wait_recv()
+            block = woall.at[core, lax.rem(chip + 4 - d, 4)]
+            stage_o.append(send(block, block, som.at[3 + d], rom.at[3 + d], (kv, mate)))
+        for c in stage_o[3:]:
+            c.wait_recv()
     with jax.named_scope("wait_e"):
         all_y, all_sq = total(xall.at[0:2032], se, re), total(sqall.at[0:127], ses, res)
         all_sq.wait_recv()
@@ -347,51 +371,56 @@
             scale = lax.rsqrt(sum_of([sqall[k * 8 + t] for t in range(8)]) / 128.0 + EPS)
             for c in range(2):
                 for n in range(4):
-                    rows = slice(((c * 16 + k) * 4 + n) * 16, ((c * 16 + k) * 4 + n) * 16 + 16)
-                    xnorm[rows, :] = (yall[c, k, n].astype(F32) * scale).astype(BF16)
+                    rows = slice(((c * 4 + n) * 16 + k) * 16, ((c * 4 + n) * 16 + k) * 16 + 16)
+                    xnorm[rows, :] = (yall[c, n, k].astype(F32) * scale).astype(BF16)
         combined = dot(woall[...].reshape(2048, 128), xnorm[...], TN)
         csend[...] = combined.reshape(8, 16, 128)
-        sqf[tp * 16 + kv] = jnp.sum(jnp.square(combined), axis=0, keepdims=True)
-    slot = sqf.at[tp * 16 + kv]
-    for a, b in everyone:
-        send(slot, slot, sh, rh, device(a, b))
+        sqf[...] = jnp.sum(jnp.square(combined), axis=0, keepdims=True)
+    for o in everyone:
+        send(sqf, sums_ref.at[tp * 16 + kv], sh, rh, device(o))
     stage_f = []
-    for b in range(1, tp_n):
-        _, t = device(0, b)
-        stage_f.append(send(csend.at[t], call.at[tp], sf.at[b], rf.at[b], (kv, t)))
-    call[tp] = csend[tp]
-    ogain = jnp.broadcast_to(row_to_column(ogain_ref[...].astype(F32)), (16, 128))
-    sums = total(sqf.at[0:127], sh, rh)
+    for b, o in enumerate(along_tp):
+        _, t = device(o)
+        stage_f.append(send(csend.at[t], comb_ref.at[tp], sf.at[b], rf.at[b], (kv, t)))
+    saves.append(pltpu.make_async_copy(sqf, sums_ref.at[tp * 16 + kv], load_sems.at[0]))
+    saves.append(pltpu.make_async_copy(csend.at[tp], comb_ref.at[tp], load_sems.at[1]))
+    for c in saves[-2:]:
+        c.start()
+    sums = total(sqall.at[0:127], sh, rh)
     with jax.named_scope("sends"):
-        for pair in stage_c:
+        for pair in stage_c + stage_w:
             for c in pair:
                 c.wait_send()
-        for c in stage_w + stage_m + stage_v + [tokens, to_mate, out_weights, out_mate, all_y, all_sq]:
+        for c in stage_wm + stage_m + stage_v + stage_o + [tokens, out_tiles, all_y, all_sq]:
             c.wait_send()
+        for c in saves:
+            c.wait()
     with jax.named_scope("wait_f"):
         for c in stage_f:
             c.wait_recv()
     with jax.named_scope("wait_h"):
         sums.wait_recv()
-    for t in range(8):
-        scale = lax.rsqrt(sum_of([sqf[t * 16 + k] for k in range(16)]) / 2048.0 + EPS)
-        out_ref[t // 2, :, (t % 2) * 128 : (t % 2) * 128 + 128] = (call[t] * scale * ogain).astype(BF16)
     for c in stage_f + [sums]:
         c.wait_send()
-    for c in saves:
-        c.wait()
-
-
-def hand_over(out_in, acc_in, out_ref, acc_ref, outv, accv, loaded, saved):
-    pieces = [(out_in, outv, out_ref)]
-    for g in range(8):
-        rows = pl.ds(g * 512, 512)
-        pieces.append((acc_in.at[rows], accv.at[rows], acc_ref.at[rows]))
-    loads = [pltpu.make_async_copy(a, b, loaded.at[n]) for n, (a, b, _) in enumerate(pieces)]
-    saves = [pltpu.make_async_copy(b, c, saved.at[n]) for n, (_, b, c) in enumerate(pieces)]
+
+
+def finish(sums_in, comb_in, gain_in, acc_in, out_ref, acc_ref, sums, comb, gain, outv, accv, loaded, saved):
+    pieces = [(sums_in, sums), (comb_in, comb), (gain_in, gain)]
+    blocks = [pl.ds(g * 512, 512) for g in range(8)]
+    pieces += [(acc_in.at[rows], accv.at[rows]) for rows in blocks]
+    loads = [pltpu.make_async_copy(a, b, loaded.at[n]) for n, (a, b) in enumerate(pieces)]
+    saves = [pltpu.make_async_copy(accv.at[rows], acc_ref.at[rows], saved.at[g]) for g, rows in enumerate(blocks)]
+    saves.append(pltpu.make_async_copy(outv, out_ref, saved.at[8]))
     for c in loads:
         c.start()
-    for load, save in zip(loads, saves):
+    for c in loads[:3]:
+        c.wait()
+    column = jnp.broadcast_to(row_to_column(gain[...].astype(F32)), (16, 128))
+    for t in range(8):
+        scale = lax.rsqrt(sum_of([sums[t * 16 + k] for k in range(16)]) / 2048.0 + EPS)
+        outv[t // 2, :, (t % 2) * 128 : (t % 2) * 128 + 128] = (comb[t] * scale * column).astype(BF16)
+    saves[8].start()
+    for load, save in zip(loads[3:], saves):
         load.wait()
         save.start()
     for c in saves:
@@ -424,9 +453,7 @@
         proposal_log_decay.transpose(1, 2, 0),
         parent.transpose(1, 0),
         head_norm_gain.reshape(1, 16),
-        output_norm_gain.reshape(1, 16),
     ]
-    vmem = pl.BlockSpec(memory_space=pltpu.VMEM)
     hbm = pl.BlockSpec(memory_space=pltpu.HBM)
     specs = [hbm] * len(args)
 
@@ -436,11 +463,15 @@
     def one():
         return [pltpu.SemaphoreType.DMA(()), pltpu.SemaphoreType.DMA(())]
 
-    out, acc = pl.pallas_call(
+    sums, combined, acc = pl.pallas_call(
         functools.partial(kernel, tp_n, kv_n),
-        out_shape=(jax.ShapeDtypeStruct((4, 16, 256), BF16), jax.ShapeDtypeStruct((4096, 128), F32)),
+        out_shape=(
+            jax.ShapeDtypeStruct((128, 1, 128), F32),
+            jax.ShapeDtypeStruct((8, 16, 128), F32),
+            jax.ShapeDtypeStruct((4096, 128), F32),
+        ),
         in_specs=specs,
-        out_specs=(vmem, hbm),
+        out_specs=(hbm, hbm, hbm),
         scratch_shapes=[
             *[pltpu.VMEM(a.shape, a.dtype) for a in args],
             pltpu.SemaphoreType.DMA((len(args),)),
@@ -448,7 +479,7 @@
             pltpu.SemaphoreType.DMA((8,)),
             pltpu.VMEM((2048, 128), BF16),
             pltpu.VMEM((2, 4, 2, 16, 2048), BF16),
-            pltpu.VMEM((2, 16, 4, 16, 128), BF16),
+            pltpu.VMEM((2, 4, 16, 16, 128), BF16),
             pltpu.VMEM((2048, 128), F32),
             pltpu.VMEM((2048, 128), BF16),
             pltpu.VMEM((8, 128, 256), BF16),
@@ -457,24 +488,31 @@
             pltpu.VMEM((8, 8, 128), F32),
             pltpu.VMEM((4096, 128), BF16),
             pltpu.VMEM((8, 16, 128), BF16),
-            pltpu.VMEM((2, 16, 4, 16, 128), BF16),
+            pltpu.VMEM((2, 4, 16, 16, 128), BF16),
             pltpu.VMEM((8, 1, 128), F32),
             pltpu.VMEM((128, 1, 128), F32),
             pltpu.VMEM((8, 16, 128), F32),
-            pltpu.VMEM((8, 16, 128), F32),
-            pltpu.VMEM((128, 1, 128), F32),
-            *one(), *sems(8), *one(), *sems(4), *sems(4), *sems(4), *sems(4), *sems(8), *one(), *one(), *one(), *one(), *sems(8), *one(),
+            pltpu.VMEM((1, 128), F32),
+            *one(), *sems(8), *sems(5), *sems(4), *sems(4), *sems(4), *sems(4), *sems(8), *one(), *sems(7), *one(), *one(), *sems(8), *one(),
         ],
         compiler_params=pltpu.CompilerParams(collective_id=0, has_side_effects=True, vmem_limit_bytes=67043328),
     )(*args)
     out, acc = pl.pallas_call(
-        hand_over,
+        finish,
         out_shape=(jax.ShapeDtypeStruct((4, 16, 256), BF16), jax.ShapeDtypeStruct((4096, 128), F32)),
-        in_specs=(hbm, hbm),
+        in_specs=(hbm,) * 4,
         out_specs=(hbm, hbm),
-        scratch_shapes=[pltpu.VMEM((4, 16, 256), BF16), pltpu.VMEM((4096, 128), F32), *sems(9)],
+        scratch_shapes=[
+            pltpu.VMEM((128, 1, 128), F32),
+            pltpu.VMEM((8, 16, 128), F32),
+            pltpu.VMEM((1, 16), BF16),
+            pltpu.VMEM((4, 16, 256), BF16),
+            pltpu.VMEM((4096, 128), F32),
+            pltpu.SemaphoreType.DMA((11,)),
+            pltpu.SemaphoreType.DMA((9,)),
+        ],
         compiler_params=pltpu.CompilerParams(vmem_limit_bytes=67043328),
-    )(out, acc)
+    )(sums, combined, output_norm_gain.reshape(1, 16), acc)
     return out.transpose(2, 0, 1), acc.reshape(256, 1, 16, 128)
 
 

time: 54.7 us -> 51.4 us (0.940)
  Pallas kernels: 53.3 us -> 49.9 us
    pallas_call x1, Pallas kernels: 50.8 us -> 47.4 us  [on_device(): pl.pallas_call(functools.partial(kernel, tp_n, kv_n), out_shape=(jax.Shap...]
where the time goes in v2:
time: 51.4 us; the launch traced here: 51.2 us
  Pallas kernels  49.9 us (97%)
  between operations  1.29 us (3%)
    pallas_call x1, Pallas kernels, on_device(): pl.pallas_call(functools.partial(kernel, tp_n, kv_n), out_shape=(jax.Shap...  47.4 us
    pallas_call x1, Pallas kernels, on_device(): pl.pallas_call(finish, out_shape=(jax.ShapeDtypeStruct((4, 16, 256), BF16...  2.53 us

profile of v2, /device:TPU:1, one launch (start us, length us, event | category | flops | bytes accessed | tf_op | source)
XLA Modules:
  0.0 51.2 jit_solution(14947396369162698300)
XLA Ops:
  1.3 47.4 %shard_map.203 = (f32[128,1,128]{2,1,0:T(1,128)}, f32[8,16,128]{2,1,0:T(8,128)}, f32[4096,128]{1,0:T(8,128)}) custom-call(bf16[4,16,256]{2,1,0:T(8,128)(2,1)} %bitcast.36, bf16[16,2048]{1,0:T(8,128)(2,1)} %bitcast.33, bf16[16,2048]{1,0:T(8,128)(2,1)} %bitcast.34, bf16[16,2048]{1,0:T(8,128)(2,1)} %bitcast.35, bf16[16,128]{1,0:T(8,128)(2,1)} %bitcast.40, ...), custom_call_target="tpu_custom_call" | custom-call | tf_op jit(solution)/shard_map/pallas_call | solution.py:466
  48.7 2.5 %shard_map.204 = (bf16[4,16,256]{2,1,0:T(8,128)(2,1)}, f32[4096,128]{1,0:T(8,128)}) custom-call(f32[128,1,128]{2,1,0:T(1,128)} %get-tuple-element.7.sums_in, f32[8,16,128]{2,1,0:T(8,128)} %get-tuple-element.8.comb_in, bf16[1,16]{1,0:T(2,128)(2,1)} %bitcast.47, f32[4096,128]{1,0:T(8,128)} %get-tuple-element.9.acc_in), custom_call_target="tpu_custom_call" | custom-call | tf_op jit(solution)/shard_map/pallas_call | solution.py:500

commit v3 on v2

--- a/solution.py
+++ b/solution.py
@@ -36,16 +36,16 @@
     return jnp.sum(jnp.where(iota((n, n), 0) == iota((n, n), 1), square, 0.0), axis=1, keepdims=True)
 
 
+def ungroup_half(parts, j):
+    chunk = iota(parts[0].shape, 1) // 32
+    total = parts[0] if j == 0 else roll(parts[0], -j * 32)
+    for m in range(1, 4):
+        total = jnp.where(chunk == m, roll(parts[m], (m - j) * 32), total)
+    return total
+
+
 def ungroup(parts, j):
-    chunk = iota(parts[0].shape, 1) // 32
-    halves = []
-    for h in range(2):
-        total = None
-        for m in range(4):
-            x = roll(parts[h * 4 + m], (m - j) * 32)
-            total = x if total is None else jnp.where(chunk == m, x, total)
-        halves.append(total)
-    return jnp.concatenate(halves, axis=1)
+    return jnp.concatenate([ungroup_half(parts[:4], j), ungroup_half(parts[4:], j)], axis=1)
 
 
 def regroup(rows, g):
@@ -119,15 +119,14 @@
 
 def new_part(accepted_state, query_key, values, beta_pre, decay_pre, rate, proposal, parent):
     reads, grams = [], []
-    for g in range(8):
-        qk = query_key(g)
-        reads.append(pick_rows(dot(accepted_state(g), qk, NT)))
+    for m in range(4):
+        qk = query_key(m)
+        reads.append(pick_rows(dot(accepted_state(m), qk, NT)))
         grams.append(pick_pairs(dot(qk, qk, NT)))
-    left = [r[:, :128] for r in reads], [r[:, 128:] for r in reads]
-    aq = [ungroup(left[0], j) for j in range(4)]
-    ak = [ungroup(left[1], j) for j in range(4)]
-    gq = [ungroup([r[:, :128] for r in grams], j) for j in range(4)]
-    gk = [ungroup([r[:, 128:] for r in grams], j) for j in range(4)]
+    aq = [ungroup_half([r[:, :128] for r in reads], j) for j in range(4)]
+    ak = [ungroup_half([r[:, 128:] for r in reads], j) for j in range(4)]
+    gq = [ungroup_half([r[:, :128] for r in grams], j) for j in range(4)]
+    gk = [ungroup_half([r[:, 128:] for r in grams], j) for j in range(4)]
     inv_q = [lax.rsqrt(gq[j][j : j + 1] + EPS) * (128.0**-0.5) for j in range(4)]
     inv_k = [lax.rsqrt(gk[j][4 + j : 5 + j] + EPS) for j in range(4)]
     ancestors = []
@@ -168,7 +167,7 @@
     xt_ref, wv_ref, wz_ref, wo_ref, gain_ref, keys_ref, state_ref, oldv_ref, logd_ref, strength_ref, accepted_ref,
     wq_ref, wk_ref, ws_ref, wd_ref, rate_ref, prop_ref, parent_ref, hgain_ref,
     load_sems, accv, acc_sems,
-    xall, wvz, woall, gaincol, xnorm, qkall, vzs, vzall, sdall, abf, ybuf, yall, sqs, sqall, csend, sqf,
+    xall, wvz, woall, gaincol, xnorm, xmate, ynorm, qkall, vzs, vzall, sdall, abf, ybuf, yall, sqs, sqall, csend, sqf,
     st, rt, sv, rv, swm, rwm, sq, rq, ssd, rsd, sqm, rqm, sdm, rdm, svz, rvz, so, ro, som, rom, se, re, ses, res, sf, rf, sh, rh,
 ):
     held = (
@@ -232,19 +231,13 @@
         send(wo_ref.at[:, cols], woall.at[core, chip, kv], so, ro, (k, tp))
     woall[core, chip, kv] = wo_ref[:, pl.ds(pl.multiple_of(kv * 128, 128), 128)]
 
-    stage_w, stage_wm = [], []
+    stage_w = []
     for d in (2, 1, 3):
         target = (kv, along_chips(d))
-        stage_w.append(
-            [
-                send(wv_ref, wvz.at[core, chip, 0], sv.at[d], rv.at[d], target),
-                send(wz_ref, wvz.at[core, chip, 1], sv.at[4 + d], rv.at[4 + d], target),
-            ]
-        )
-    stage_wm.append(send(wv_ref, wvz.at[core, chip, 0], swm.at[0], rwm.at[0], (kv, mate)))
-    stage_wm.append(send(wz_ref, wvz.at[core, chip, 1], swm.at[4], rwm.at[4], (kv, mate)))
-    wvz[core, chip, 0] = wv_ref[...]
-    wvz[core, chip, 1] = wz_ref[...]
+        stage_w.append(send(wv_ref, wvz.at[chip, 0], sv.at[d], rv.at[d], target))
+        stage_w.append(send(wz_ref, wvz.at[chip, 1], sv.at[4 + d], rv.at[4 + d], target))
+    wvz[chip, 0] = wv_ref[...]
+    wvz[chip, 1] = wz_ref[...]
     for n in range(16):
         column = row_to_column(gain_ref[n : n + 1, :].astype(F32))
         gaincol[n * 128 : n * 128 + 128, :] = jnp.broadcast_to(column, (128, 128))
@@ -290,22 +283,26 @@
         target = (kv, along_chips(d))
         stage_c.append((send(qkall.at[tp], qkall.at[tp], sq.at[d], rq.at[d], target), send(sdall.at[tp], sdall.at[tp], ssd.at[d], rsd.at[d], target)))
     stage_m = [send(qkall.at[tp], qkall.at[tp], sqm.at[0], rqm.at[0], (kv, mate)), send(sdall.at[tp], sdall.at[tp], sdm.at[0], rdm.at[0], (kv, mate))]
+    to_mate = send(xnorm, xmate, swm, rwm, (kv, mate))
     with jax.named_scope("wait_w"):
-        for d, pair in ((1, stage_w[1]), (3, stage_w[2]), (2, stage_w[0])):
-            for c in pair:
-                c.wait_recv()
-            block = wvz.at[core, lax.rem(chip + 4 - d, 4)]
-            stage_wm.append(send(block, block, swm.at[d], rwm.at[d], (kv, mate)))
+        for c in stage_w:
+            c.wait_recv()
     with jax.named_scope("wait_wm"):
-        for c in stage_wm:
-            c.wait_recv()
-    vzs[...] = dot(wvz[...].reshape(256, 2048), xnorm[...]).astype(BF16).reshape(8, 2, 16, 128)
+        to_mate.wait_recv()
+    weights = wvz[...].reshape(128, 2048)
+    for h, rows in ((core, xnorm), (1 - core, xmate)):
+        product = dot(weights, rows[...]).astype(BF16).reshape(4, 2, 16, 128)
+        for n in range(4):
+            vzs[n, h] = product[n]
     stage_v = []
-    along_tp = far_first(itertools.product([0], [0], range(4), range(2)))
-    for b, o in enumerate(along_tp):
-        _, t = device(o)
-        stage_v.append(send(vzs.at[lax.rem(t, 2) * 4 + t // 2], vzall.at[tp], svz.at[b], rvz.at[b], (kv, t)))
-    vzall[tp] = vzs[core * 4 + chip]
+    for d in (2, 1, 3):
+        stage_v.append(send(vzs.at[lax.rem(chip + d, 4)], vzall.at[chip], svz.at[d], rvz.at[d], (kv, along_chips(d))))
+    vzall[chip] = vzs[chip]
+    out_tiles = total(xall.at[0:240], so, ro)
+    out_tiles.wait_recv()
+    block = woall.at[core, chip]
+    stage_o = [send(block, block, som.at[d], rom.at[d], (kv, along_chips(d))) for d in (2, 1, 3)]
+    stage_o.append(send(block, block, som.at[0], rom.at[0], (kv, mate)))
     with jax.named_scope("wait_c"):
         for d, pair in ((1, stage_c[1]), (3, stage_c[2]), (2, stage_c[0])):
             for c in pair:
@@ -313,48 +310,46 @@
             source = lax.rem(chip + 4 - d, 4) * 2 + core
             stage_m.append(send(qkall.at[source], qkall.at[source], sqm.at[d], rqm.at[d], (kv, mate)))
             stage_m.append(send(sdall.at[source], sdall.at[source], sdm.at[d], rdm.at[d], (kv, mate)))
-    out_tiles = total(xall.at[0:240], so, ro)
-    out_tiles.wait_recv()
-    block = woall.at[core, chip]
-    stage_o = [send(block, block, som.at[d], rom.at[d], (kv, along_chips(d))) for d in (2, 1, 3)]
-    stage_o.append(send(block, block, som.at[0], rom.at[0], (kv, mate)))
-    with jax.named_scope("wait_m"):
-        for c in stage_m + stage_v:
+    with jax.named_scope("wait_v"):
+        for c in stage_v:
             c.wait_recv()
-
-    def query_key(g):
-        h, m = divmod(g, 4)
-        pieces = [qkall[p * 2 + h, m * 32 : m * 32 + 32, s * 128 : s * 128 + 128] for s in range(2) for p in range(4)]
-        return jnp.concatenate(pieces, axis=0)
-
-    def both(f):
-        return [jnp.concatenate([f(p * 2), f(p * 2 + 1)], axis=1) for p in range(4)]
-
-    with jax.named_scope("new"):
+    hgain = jnp.broadcast_to(row_to_column(hgain_ref[...].astype(F32)), (16, 128))
+
+    def half(h, offsets):
+        lanes = pl.ds(pl.multiple_of(h * 128, 128), 128)
+
+        def query_key(m):
+            pieces = [qkall[p * 2 + h, m * 32 : m * 32 + 32, s * 128 : s * 128 + 128] for s in range(2) for p in range(4)]
+            return jnp.concatenate(pieces, axis=0)
+
         outputs = new_part(
-            lambda g: abf[g * 512 : g * 512 + 512, :],
+            lambda m: abf[pl.ds(pl.multiple_of((h * 4 + m) * 512, 512), 512), :],
             query_key,
-            both(lambda t: vzall[t, 0].astype(F32)),
-            both(lambda t: sdall[t, 0:1, :]),
-            both(lambda t: sdall[t, 1:2, :]),
+            [vzall[p, h, 0].astype(F32) for p in range(4)],
+            [sdall[p * 2 + h, 0:1, :] for p in range(4)],
+            [sdall[p * 2 + h, 1:2, :] for p in range(4)],
             rate_ref[...],
-            [prop_ref[j] for j in range(4)],
-            [parent_ref[j : j + 1, :] for j in range(4)],
+            [prop_ref[j, :, lanes] for j in range(4)],
+            [parent_ref[j : j + 1, lanes] for j in range(4)],
         )
-        zgate = both(lambda t: vzall[t, 1].astype(F32))
-        hgain = jnp.broadcast_to(row_to_column(hgain_ref[...].astype(F32)), (16, 256))
-        for t in range(8):
-            half = slice((t % 2) * 128, (t % 2) * 128 + 128)
-            o, z = outputs[t // 2][:, half], zgate[t // 2][:, half]
-            sqs[t] = jnp.sum(jnp.square(o), axis=0, keepdims=True)
-            ybuf[t] = (o * hgain[:, half] * (z * jax.nn.sigmoid(z))).astype(BF16)
-    with jax.named_scope("issue_e"):
-        for o in everyone:
+        for p in range(4):
+            o, z = outputs[p], vzall[p, h, 1].astype(F32)
+            sqs[p * 2 + h] = jnp.sum(jnp.square(o), axis=0, keepdims=True)
+            ybuf[p * 2 + h] = (o * hgain * (z * jax.nn.sigmoid(z))).astype(BF16)
+        for o in offsets:
             k, t = device(o)
             send(sqs.at[t], sqall.at[own], ses, res, (k, t))
             send(ybuf.at[t], yall.at[core, chip, kv], se, re, (k, t))
-        sqall[own] = sqs[tp]
-        yall[core, chip, kv] = ybuf[tp]
+
+    with jax.named_scope("new1"):
+        half(core, [o for o in everyone if o[3] == 0])
+    sqall[own] = sqs[tp]
+    yall[core, chip, kv] = ybuf[tp]
+    with jax.named_scope("wait_m"):
+        for c in stage_m:
+            c.wait_recv()
+    with jax.named_scope("new2"):
+        half(1 - core, [o for o in everyone if o[3] == 1])
     with jax.named_scope("wait_o"):
         for d, c in ((1, stage_o[1]), (3, stage_o[2]), (2, stage_o[0])):
             c.wait_recv()
@@ -372,14 +367,14 @@
             for c in range(2):
                 for n in range(4):
                     rows = slice(((c * 4 + n) * 16 + k) * 16, ((c * 4 + n) * 16 + k) * 16 + 16)
-                    xnorm[rows, :] = (yall[c, n, k].astype(F32) * scale).astype(BF16)
-        combined = dot(woall[...].reshape(2048, 128), xnorm[...], TN)
+                    ynorm[rows, :] = (yall[c, n, k].astype(F32) * scale).astype(BF16)
+        combined = dot(woall[...].reshape(2048, 128), ynorm[...], TN)
         csend[...] = combined.reshape(8, 16, 128)
         sqf[...] = jnp.sum(jnp.square(combined), axis=0, keepdims=True)
     for o in everyone:
         send(sqf, sums_ref.at[tp * 16 + kv], sh, rh, device(o))
     stage_f = []
-    for b, o in enumerate(along_tp):
+    for b, o in enumerate(far_first(itertools.product([0], [0], range(4), range(2)))):
         _, t = device(o)
         stage_f.append(send(csend.at[t], comb_ref.at[tp], sf.at[b], rf.at[b], (kv, t)))
     saves.append(pltpu.make_async_copy(sqf, sums_ref.at[tp * 16 + kv], load_sems.at[0]))
@@ -388,10 +383,10 @@
         c.start()
     sums = total(sqall.at[0:127], sh, rh)
     with jax.named_scope("sends"):
-        for pair in stage_c + stage_w:
+        for pair in stage_c:
             for c in pair:
                 c.wait_send()
-        for c in stage_wm + stage_m + stage_v + stage_o + [tokens, out_tiles, all_y, all_sq]:
+        for c in stage_w + stage_m + stage_v + stage_o + [to_mate, tokens, out_tiles, all_y, all_sq]:
             c.wait_send()
         for c in saves:
             c.wait()
@@ -478,13 +473,15 @@
             pltpu.VMEM((4096, 128), F32),
             pltpu.SemaphoreType.DMA((8,)),
             pltpu.VMEM((2048, 128), BF16),
-            pltpu.VMEM((2, 4, 2, 16, 2048), BF16),
+            pltpu.VMEM((4, 2, 16, 2048), BF16),
             pltpu.VMEM((2, 4, 16, 16, 128), BF16),
             pltpu.VMEM((2048, 128), F32),
             pltpu.VMEM((2048, 128), BF16),
+            pltpu.VMEM((2048, 128), BF16),
+            pltpu.VMEM((2048, 128), BF16),
             pltpu.VMEM((8, 128, 256), BF16),
-            pltpu.VMEM((8, 2, 16, 128), BF16),
-            pltpu.VMEM((8, 2, 16, 128), BF16),
+            pltpu.VMEM((4, 2, 2, 16, 128), BF16),
+            pltpu.VMEM((4, 2, 2, 16, 128), BF16),
             pltpu.VMEM((8, 8, 128), F32),
             pltpu.VMEM((4096, 128), BF16),
             pltpu.VMEM((8, 16, 128), BF16),
@@ -493,7 +490,7 @@
             pltpu.VMEM((128, 1, 128), F32),
             pltpu.VMEM((8, 16, 128), F32),
             pltpu.VMEM((1, 128), F32),
-            *one(), *sems(8), *sems(5), *sems(4), *sems(4), *sems(4), *sems(4), *sems(8), *one(), *sems(7), *one(), *one(), *sems(8), *one(),
+            *one(), *sems(8), *one(), *sems(4), *sems(4), *sems(4), *sems(4), *sems(4), *one(), *sems(7), *one(), *one(), *sems(8), *one(),
         ],
         compiler_params=pltpu.CompilerParams(collective_id=0, has_side_effects=True, vmem_limit_bytes=67043328),
     )(*args)

time: 51.4 us -> 49.1 us (0.955)
  Pallas kernels: 49.9 us -> 47.7 us
    pallas_call x1, Pallas kernels: 47.4 us -> 45.1 us  [on_device(): pl.pallas_call(functools.partial(kernel, tp_n, kv_n), out_shape=(jax.Shap...]
where the time goes in v3:
time: 49.1 us; the launch traced here: 49 us
  Pallas kernels  47.7 us (97%)
  between operations  1.29 us (3%)
    pallas_call x1, Pallas kernels, on_device(): pl.pallas_call(functools.partial(kernel, tp_n, kv_n), out_shape=(jax.Shap...  45.1 us
    pallas_call x1, Pallas kernels, on_device(): pl.pallas_call(finish, out_shape=(jax.ShapeDtypeStruct((4, 16, 256), BF16...  2.53 us

profile of v3, /device:TPU:1, one launch (start us, length us, event | category | flops | bytes accessed | tf_op | source)
XLA Modules:
  0.0 49.0 jit_solution(8689504458979847475)
XLA Ops:
  1.3 45.1 %shard_map.203 = (f32[128,1,128]{2,1,0:T(1,128)}, f32[8,16,128]{2,1,0:T(8,128)}, f32[4096,128]{1,0:T(8,128)}) custom-call(bf16[4,16,256]{2,1,0:T(8,128)(2,1)} %bitcast.36, bf16[16,2048]{1,0:T(8,128)(2,1)} %bitcast.33, bf16[16,2048]{1,0:T(8,128)(2,1)} %bitcast.34, bf16[16,2048]{1,0:T(8,128)(2,1)} %bitcast.35, bf16[16,128]{1,0:T(8,128)(2,1)} %bitcast.40, ...), custom_call_target="tpu_custom_call" | custom-call | tf_op jit(solution)/shard_map/pallas_call | solution.py:461
  46.4 2.5 %shard_map.204 = (bf16[4,16,256]{2,1,0:T(8,128)(2,1)}, f32[4096,128]{1,0:T(8,128)}) custom-call(f32[128,1,128]{2,1,0:T(1,128)} %get-tuple-element.7.sums_in, f32[8,16,128]{2,1,0:T(8,128)} %get-tuple-element.8.comb_in, bf16[1,16]{1,0:T(2,128)(2,1)} %bitcast.47, f32[4096,128]{1,0:T(8,128)} %get-tuple-element.9.acc_in), custom_call_target="tpu_custom_call" | custom-call | tf_op jit(solution)/shard_map/pallas_call | solution.py:497

commit v4 on v3

--- a/solution.py
+++ b/solution.py
@@ -117,7 +117,7 @@
         store(g, scale * state(g) + dot(block, grouped[g]))
 
 
-def new_part(accepted_state, query_key, values, beta_pre, decay_pre, rate, proposal, parent):
+def new_reads(accepted_state, query_key):
     reads, grams = [], []
     for m in range(4):
         qk = query_key(m)
@@ -129,6 +129,11 @@
     gk = [ungroup_half([r[:, 128:] for r in grams], j) for j in range(4)]
     inv_q = [lax.rsqrt(gq[j][j : j + 1] + EPS) * (128.0**-0.5) for j in range(4)]
     inv_k = [lax.rsqrt(gk[j][4 + j : 5 + j] + EPS) for j in range(4)]
+    return aq, ak, gk, inv_q, inv_k
+
+
+def new_part(products, values, beta_pre, decay_pre, rate, proposal, parent):
+    aq, ak, gk, inv_q, inv_k = products
     ancestors = []
     for i in range(4):
         row = {j: (parent[i] == j).astype(F32) for j in range(i)}
@@ -168,7 +173,7 @@
     wq_ref, wk_ref, ws_ref, wd_ref, rate_ref, prop_ref, parent_ref, hgain_ref,
     load_sems, accv, acc_sems,
     xall, wvz, woall, gaincol, xnorm, xmate, ynorm, qkall, vzs, vzall, sdall, abf, ybuf, yall, sqs, sqall, csend, sqf,
-    st, rt, sv, rv, swm, rwm, sq, rq, ssd, rsd, sqm, rqm, sdm, rdm, svz, rvz, so, ro, som, rom, se, re, ses, res, sf, rf, sh, rh,
+    sa, ra, st, rt, sv, rv, swm, rwm, sq, rq, ssd, rsd, sqm, rqm, sdm, rdm, svz, rvz, so, ro, som, rom, se, re, ses, res, sf, rf, sh, rh,
 ):
     held = (
         xt_ref, wv_ref, wz_ref, wo_ref, gain_ref, keys_ref, state_ref, oldv_ref, logd_ref, strength_ref, accepted_ref,
@@ -208,28 +213,32 @@
     barrier = pltpu.get_barrier_semaphore()
     for c in loads[:5]:
         c.start()
-    for o in everyone:
+    plane = far_first(itertools.product(range(4), range(4), [0], [0]))
+    line = far_first(itertools.product([0], [0], range(4), range(2)))
+    for o in plane + line:
         pl.semaphore_signal(barrier, inc=1, device_id=device(o), device_id_type=MESH)
     for c in loads[5:]:
         c.start()
     for c in loads[:5]:
         c.wait()
     with jax.named_scope("barrier"):
-        pl.semaphore_wait(barrier, kv_n * tp_n - 1)
-
+        pl.semaphore_wait(barrier, kv_n - 1 + tp_n - 1)
+
+    def hand_on(first, count):
+        rows = pl.ds(pl.multiple_of((kv * tp_n + first) * 16, 16), count * 16)
+        for o in plane:
+            send(xall.at[rows], xall.at[rows], st, rt, device(o))
+
+    own_rows = pl.ds(pl.multiple_of(own * 16, 16), 16)
+    stage_a = {}
     with jax.named_scope("issue_t"):
-        own_rows = pl.ds(pl.multiple_of(own * 16, 16), 16)
-        for o in everyone:
-            k, t = device(o)
-            send(xt_ref.at[t // 2, :, lanes_of(t)], xall.at[own_rows], st, rt, (k, t))
+        for b, o in enumerate(line):
+            _, t = device(o)
+            stage_a[o[2:]] = send(xt_ref.at[t // 2, :, lanes_of(t)], xall.at[own_rows], sa.at[b], ra.at[b], (kv, t))
         xall[own_rows, :] = xt_ref[tp // 2, :, lanes_of(tp)]
-        tokens = total(xall.at[0:2032], st, rt)
-
-    for o in far_first(itertools.product(range(4), range(4), [0], [0])):
-        k, _ = device(o)
-        cols = pl.ds(pl.multiple_of(k * 128, 128), 128)
-        send(wo_ref.at[:, cols], woall.at[core, chip, kv], so, ro, (k, tp))
-    woall[core, chip, kv] = wo_ref[:, pl.ds(pl.multiple_of(kv * 128, 128), 128)]
+        own_tile = xt_ref.at[tp // 2, :, lanes_of(tp)]
+        for o in plane:
+            send(own_tile, xall.at[own_rows], st, rt, device(o))
 
     stage_w = []
     for d in (2, 1, 3):
@@ -238,9 +247,22 @@
         stage_w.append(send(wz_ref, wvz.at[chip, 1], sv.at[4 + d], rv.at[4 + d], target))
     wvz[chip, 0] = wv_ref[...]
     wvz[chip, 1] = wz_ref[...]
+    for o in plane:
+        k, _ = device(o)
+        cols = pl.ds(pl.multiple_of(k * 128, 128), 128)
+        send(wo_ref.at[:, cols], woall.at[core, chip, kv], so, ro, (k, tp))
+    woall[core, chip, kv] = wo_ref[:, pl.ds(pl.multiple_of(kv * 128, 128), 128)]
     for n in range(16):
         column = row_to_column(gain_ref[n : n + 1, :].astype(F32))
         gaincol[n * 128 : n * 128 + 128, :] = jnp.broadcast_to(column, (128, 128))
+    with jax.named_scope("wait_a"):
+        stage_a[0, 1].wait_recv()
+        hand_on(mate, 1)
+        for d in (1, 3, 2):
+            for c in range(2):
+                stage_a[d, c].wait_recv()
+            hand_on(lax.rem(chip + 4 - d, 4) * 2, 2)
+    tokens = total(xall.at[0:1920], st, rt)
     for c in loads[5:]:
         c.wait()
 
@@ -264,6 +286,11 @@
             store,
         )
 
+    out_tiles = total(xall.at[0:240], so, ro)
+    out_tiles.wait_recv()
+    block = woall.at[core, chip]
+    stage_o = [send(block, block, som.at[d], rom.at[d], (kv, along_chips(d))) for d in (2, 1, 3)]
+    stage_o.append(send(block, block, som.at[0], rom.at[0], (kv, mate)))
     with jax.named_scope("wait_t"):
         tokens.wait_recv()
     with jax.named_scope("project"):
@@ -298,11 +325,6 @@
     for d in (2, 1, 3):
         stage_v.append(send(vzs.at[lax.rem(chip + d, 4)], vzall.at[chip], svz.at[d], rvz.at[d], (kv, along_chips(d))))
     vzall[chip] = vzs[chip]
-    out_tiles = total(xall.at[0:240], so, ro)
-    out_tiles.wait_recv()
-    block = woall.at[core, chip]
-    stage_o = [send(block, block, som.at[d], rom.at[d], (kv, along_chips(d))) for d in (2, 1, 3)]
-    stage_o.append(send(block, block, som.at[0], rom.at[0], (kv, mate)))
     with jax.named_scope("wait_c"):
         for d, pair in ((1, stage_c[1]), (3, stage_c[2]), (2, stage_c[0])):
             for c in pair:
@@ -310,21 +332,19 @@
             source = lax.rem(chip + 4 - d, 4) * 2 + core
             stage_m.append(send(qkall.at[source], qkall.at[source], sqm.at[d], rqm.at[d], (kv, mate)))
             stage_m.append(send(sdall.at[source], sdall.at[source], sdm.at[d], rdm.at[d], (kv, mate)))
-    with jax.named_scope("wait_v"):
-        for c in stage_v:
-            c.wait_recv()
     hgain = jnp.broadcast_to(row_to_column(hgain_ref[...].astype(F32)), (16, 128))
 
-    def half(h, offsets):
-        lanes = pl.ds(pl.multiple_of(h * 128, 128), 128)
-
+    def reads_of(h):
         def query_key(m):
             pieces = [qkall[p * 2 + h, m * 32 : m * 32 + 32, s * 128 : s * 128 + 128] for s in range(2) for p in range(4)]
             return jnp.concatenate(pieces, axis=0)
 
+        return new_reads(lambda m: abf[pl.ds(pl.multiple_of((h * 4 + m) * 512, 512), 512), :], query_key)
+
+    def half(h, products, offsets):
+        lanes = pl.ds(pl.multiple_of(h * 128, 128), 128)
         outputs = new_part(
-            lambda m: abf[pl.ds(pl.multiple_of((h * 4 + m) * 512, 512), 512), :],
-            query_key,
+            products,
             [vzall[p, h, 0].astype(F32) for p in range(4)],
             [sdall[p * 2 + h, 0:1, :] for p in range(4)],
             [sdall[p * 2 + h, 1:2, :] for p in range(4)],
@@ -341,15 +361,20 @@
             send(sqs.at[t], sqall.at[own], ses, res, (k, t))
             send(ybuf.at[t], yall.at[core, chip, kv], se, re, (k, t))
 
+    with jax.named_scope("reads1"):
+        products = reads_of(core)
+    with jax.named_scope("wait_v"):
+        for c in stage_v:
+            c.wait_recv()
     with jax.named_scope("new1"):
-        half(core, [o for o in everyone if o[3] == 0])
+        half(core, products, [o for o in everyone if o[3] == 0])
     sqall[own] = sqs[tp]
     yall[core, chip, kv] = ybuf[tp]
     with jax.named_scope("wait_m"):
         for c in stage_m:
             c.wait_recv()
     with jax.named_scope("new2"):
-        half(1 - core, [o for o in everyone if o[3] == 1])
+        half(1 - core, reads_of(1 - core), [o for o in everyone if o[3] == 1])
     with jax.named_scope("wait_o"):
         for d, c in ((1, stage_o[1]), (3, stage_o[2]), (2, stage_o[0])):
             c.wait_recv()
@@ -374,7 +399,7 @@
     for o in everyone:
         send(sqf, sums_ref.at[tp * 16 + kv], sh, rh, device(o))
     stage_f = []
-    for b, o in enumerate(far_first(itertools.product([0], [0], range(4), range(2)))):
+    for b, o in enumerate(line):
         _, t = device(o)
         stage_f.append(send(csend.at[t], comb_ref.at[tp], sf.at[b], rf.at[b], (kv, t)))
     saves.append(pltpu.make_async_copy(sqf, sums_ref.at[tp * 16 + kv], load_sems.at[0]))
@@ -386,7 +411,7 @@
         for pair in stage_c:
             for c in pair:
                 c.wait_send()
-        for c in stage_w + stage_m + stage_v + stage_o + [to_mate, tokens, out_tiles, all_y, all_sq]:
+        for c in list(stage_a.values()) + stage_w + stage_m + stage_v + stage_o + [to_mate, tokens, out_tiles, all_y, all_sq]:
             c.wait_send()
         for c in saves:
             c.wait()
@@ -490,7 +515,7 @@
             pltpu.VMEM((128, 1, 128), F32),
             pltpu.VMEM((8, 16, 128), F32),
             pltpu.VMEM((1, 128), F32),
-            *one(), *sems(8), *one(), *sems(4), *sems(4), *sems(4), *sems(4), *sems(4), *one(), *sems(7), *one(), *one(), *sems(8), *one(),
+            *sems(8), *one(), *sems(8), *one(), *sems(4), *sems(4), *sems(4), *sems(4), *sems(4), *one(), *sems(7), *one(), *one(), *sems(8), *one(),
         ],
         compiler_params=pltpu.CompilerParams(collective_id=0, has_side_effects=True, vmem_limit_bytes=67043328),
     )(*args)

time: 49.1 us -> 47.3 us (0.963)
  Pallas kernels: 47.7 us -> 45.8 us
    pallas_call x1, Pallas kernels: 45.1 us -> 43.3 us  [on_device(): pl.pallas_call(functools.partial(kernel, tp_n, kv_n), out_shape=(jax.Shap...]
where the time goes in v4:
time: 47.3 us; the launch traced here: 47.1 us
  Pallas kernels  45.8 us (97%)
  between operations  1.29 us (3%)
    pallas_call x1, Pallas kernels, on_device(): pl.pallas_call(functools.partial(kernel, tp_n, kv_n), out_shape=(jax.Shap...  43.3 us
    pallas_call x1, Pallas kernels, on_device(): pl.pallas_call(finish, out_shape=(jax.ShapeDtypeStruct((4, 16, 256), BF16...  2.53 us

profile of v4, /device:TPU:1, one launch (start us, length us, event | category | flops | bytes accessed | tf_op | source)
XLA Modules:
  0.0 47.1 jit_solution(1187698863467284258)
XLA Ops:
  1.3 43.3 %shard_map.203 = (f32[128,1,128]{2,1,0:T(1,128)}, f32[8,16,128]{2,1,0:T(8,128)}, f32[4096,128]{1,0:T(8,128)}) custom-call(bf16[4,16,256]{2,1,0:T(8,128)(2,1)} %bitcast.36, bf16[16,2048]{1,0:T(8,128)(2,1)} %bitcast.33, bf16[16,2048]{1,0:T(8,128)(2,1)} %bitcast.34, bf16[16,2048]{1,0:T(8,128)(2,1)} %bitcast.35, bf16[16,128]{1,0:T(8,128)(2,1)} %bitcast.40, ...), custom_call_target="tpu_custom_call" | custom-call | tf_op jit(solution)/shard_map/pallas_call | solution.py:486
  44.6 2.5 %shard_map.204 = (bf16[4,16,256]{2,1,0:T(8,128)(2,1)}, f32[4096,128]{1,0:T(8,128)}) custom-call(f32[128,1,128]{2,1,0:T(1,128)} %get-tuple-element.7.sums_in, f32[8,16,128]{2,1,0:T(8,128)} %get-tuple-element.8.comb_in, bf16[1,16]{1,0:T(2,128)(2,1)} %bitcast.47, f32[4096,128]{1,0:T(8,128)} %get-tuple-element.9.acc_in), custom_call_target="tpu_custom_call" | custom-call | tf_op jit(solution)/shard_map/pallas_call | solution.py:522

commit v5 on v4

--- a/solution.py
+++ b/solution.py
@@ -118,13 +118,14 @@
 
 
 def new_reads(accepted_state, query_key):
-    reads, grams = [], []
+    reads, grams = ([], []), []
     for m in range(4):
         qk = query_key(m)
-        reads.append(pick_rows(dot(accepted_state(m), qk, NT)))
+        for c, state in enumerate(accepted_state(m)):
+            reads[c].append(pick_rows(dot(state, qk, NT)))
         grams.append(pick_pairs(dot(qk, qk, NT)))
-    aq = [ungroup_half([r[:, :128] for r in reads], j) for j in range(4)]
-    ak = [ungroup_half([r[:, 128:] for r in reads], j) for j in range(4)]
+    aq = [[ungroup_half([r[:, :128] for r in reads[c]], j) for j in range(4)] for c in range(2)]
+    ak = [[ungroup_half([r[:, 128:] for r in reads[c]], j) for j in range(4)] for c in range(2)]
     gq = [ungroup_half([r[:, :128] for r in grams], j) for j in range(4)]
     gk = [ungroup_half([r[:, 128:] for r in grams], j) for j in range(4)]
     inv_q = [lax.rsqrt(gq[j][j : j + 1] + EPS) * (128.0**-0.5) for j in range(4)]
@@ -146,18 +147,18 @@
         g_new.append(-rate * softplus + proposal[i])
         beta.append(jax.nn.sigmoid(beta_pre[i]))
         gam.append(sum_of([g_new[i]] + [ancestors[i][j] * g_new[j] for j in range(i)]))
-    outputs, update = [], []
+    outputs, update = ([], []), ([], [])
     for i in range(4):
         grow = jnp.exp(gam[i])
-        u = beta[i] * (values[i] - (grow * inv_k[i]) * ak[i])
-        o = (grow * inv_q[i]) * aq[i]
-        for j in range(i):
-            reach = jnp.exp(jnp.minimum(gam[i] - gam[j], 0.0)) * ancestors[i][j] * inv_k[j]
-            u = u - (beta[i] * inv_k[i] * gk[j][4 + i : 5 + i] * reach) * update[j]
-            o = o + (inv_q[i] * gk[j][i : i + 1] * reach) * update[j]
-        update.append(u)
-        o = o + (inv_q[i] * gk[i][i : i + 1] * inv_k[i]) * u
-        outputs.append(o)
+        reach = [jnp.exp(jnp.minimum(gam[i] - gam[j], 0.0)) * ancestors[i][j] * inv_k[j] for j in range(i)]
+        for c in range(2):
+            u = beta[i] * (values[c][i] - (grow * inv_k[i]) * ak[c][i])
+            o = (grow * inv_q[i]) * aq[c][i]
+            for j in range(i):
+                u = u - (beta[i] * inv_k[i] * gk[j][4 + i : 5 + i] * reach[j]) * update[c][j]
+                o = o + (inv_q[i] * gk[j][i : i + 1] * reach[j]) * update[c][j]
+            update[c].append(u)
+            outputs[c].append(o + (inv_q[i] * gk[i][i : i + 1] * inv_k[i]) * u)
     return outputs
 
 
@@ -171,9 +172,9 @@
     tp_n, kv_n, sources, sums_ref, comb_ref, acc_ref,
     xt_ref, wv_ref, wz_ref, wo_ref, gain_ref, keys_ref, state_ref, oldv_ref, logd_ref, strength_ref, accepted_ref,
     wq_ref, wk_ref, ws_ref, wd_ref, rate_ref, prop_ref, parent_ref, hgain_ref,
-    load_sems, accv, acc_sems,
-    xall, wvz, woall, gaincol, xnorm, xmate, ynorm, qkall, vzs, vzall, sdall, abf, ybuf, yall, sqs, sqall, csend, sqf,
-    sa, ra, st, rt, sv, rv, swm, rwm, sq, rq, ssd, rsd, sqm, rqm, sdm, rdm, svz, rvz, so, ro, som, rom, se, re, ses, res, sf, rf, sh, rh,
+    load_sems, accv, acc_sem,
+    xall, wvz, woall, gaincol, hgcol, xnorm, ynorm, qkall, vzs, vzall, sdall, abf, amate, ybuf, yall, sqs, sqall, csend, sqf,
+    sa, ra, st, rt, sv, rv, swm, rwm, sq, rq, svz, rvz, so, ro, som, rom, se, re, ses, res, sf, rf, sh, rh,
 ):
     held = (
         xt_ref, wv_ref, wz_ref, wo_ref, gain_ref, keys_ref, state_ref, oldv_ref, logd_ref, strength_ref, accepted_ref,
@@ -240,21 +241,23 @@
         for o in plane:
             send(own_tile, xall.at[own_rows], st, rt, device(o))
 
-    stage_w = []
     for d in (2, 1, 3):
         target = (kv, along_chips(d))
-        stage_w.append(send(wv_ref, wvz.at[chip, 0], sv.at[d], rv.at[d], target))
-        stage_w.append(send(wz_ref, wvz.at[chip, 1], sv.at[4 + d], rv.at[4 + d], target))
-    wvz[chip, 0] = wv_ref[...]
-    wvz[chip, 1] = wz_ref[...]
+        send(wv_ref, wvz.at[core, chip, 0], sv.at[0], rv.at[0], target)
+        send(wz_ref, wvz.at[core, chip, 1], sv.at[1], rv.at[1], target)
+    stage_w = [total(wvz.at[core, 0:3, n], sv.at[n], rv.at[n]) for n in range(2)]
+    wvz[core, chip, 0] = wv_ref[...]
+    wvz[core, chip, 1] = wz_ref[...]
     for o in plane:
         k, _ = device(o)
         cols = pl.ds(pl.multiple_of(k * 128, 128), 128)
-        send(wo_ref.at[:, cols], woall.at[core, chip, kv], so, ro, (k, tp))
-    woall[core, chip, kv] = wo_ref[:, pl.ds(pl.multiple_of(kv * 128, 128), 128)]
+        send(wo_ref.at[:, cols], woall.at[chip, kv, core], so, ro, (k, tp))
+    woall[chip, kv, core] = wo_ref[:, pl.ds(pl.multiple_of(kv * 128, 128), 128)]
+    loads[18].wait()
     for n in range(16):
         column = row_to_column(gain_ref[n : n + 1, :].astype(F32))
         gaincol[n * 128 : n * 128 + 128, :] = jnp.broadcast_to(column, (128, 128))
+    hgcol[core] = jnp.broadcast_to(row_to_column(hgain_ref[...].astype(F32)), (16, 128))
     with jax.named_scope("wait_a"):
         stage_a[0, 1].wait_recv()
         hand_on(mate, 1)
@@ -263,7 +266,7 @@
                 stage_a[d, c].wait_recv()
             hand_on(lax.rem(chip + 4 - d, 4) * 2, 2)
     tokens = total(xall.at[0:1920], st, rt)
-    for c in loads[5:]:
+    for c in loads[5:18]:
         c.wait()
 
     saves = []
@@ -271,8 +274,6 @@
     def store(g, value):
         rows = slice(g * 512, g * 512 + 512)
         accv[rows, :] = value
-        saves.append(pltpu.make_async_copy(accv.at[rows], acc_ref.at[rows], acc_sems.at[g]))
-        saves[-1].start()
         abf[g * 512 : g * 512 + 512, :] = value.astype(BF16)
 
     with jax.named_scope("old"):
@@ -286,11 +287,20 @@
             store,
         )
 
+    saves.append(pltpu.make_async_copy(accv, acc_ref, acc_sem))
+    saves[-1].start()
     out_tiles = total(xall.at[0:240], so, ro)
     out_tiles.wait_recv()
-    block = woall.at[core, chip]
-    stage_o = [send(block, block, som.at[d], rom.at[d], (kv, along_chips(d))) for d in (2, 1, 3)]
-    stage_o.append(send(block, block, som.at[0], rom.at[0], (kv, mate)))
+    block = woall.at[chip, :, core]
+    for d in (2, 1, 3):
+        send(block, block, som.at[1], rom.at[1], (kv, along_chips(d)))
+    stage_o = [total(woall.at[0:3, :, core], som.at[1], rom.at[1])]
+    theirs = pl.ds(pl.multiple_of((1 - core) * 2048, 2048), 2048)
+    to_mate = [send(abf.at[theirs], amate, swm.at[0], rwm.at[0], (kv, mate)), send(hgcol.at[core], hgcol.at[core], swm.at[1], rwm.at[1], (kv, mate))]
+    with jax.named_scope("wait_w"):
+        for c in stage_w:
+            c.wait_recv()
+    to_mate.append(send(wvz.at[core], wvz.at[core], swm.at[2], rwm.at[2], (kv, mate)))
     with jax.named_scope("wait_t"):
         tokens.wait_recv()
     with jax.named_scope("project"):
@@ -300,118 +310,105 @@
             rows = slice(n * 128, n * 128 + 128)
             xnorm[rows, :] = (xall[rows, :].astype(F32) * scale * gaincol[rows, :]).astype(BF16)
         x = xnorm[...]
-        qkall[tp, :, 0:128] = dot(x, wq_ref[...], TN).astype(BF16)
-        qkall[tp, :, 128:256] = dot(x, wk_ref[...], TN).astype(BF16)
+        qkall[0, chip] = dot(x, wq_ref[...], TN).astype(BF16)
+        for d in (2, 1, 3):
+            send(qkall.at[0, chip], qkall.at[0, chip], sq.at[0], rq.at[0], (kv, along_chips(d)))
+        qkall[1, chip] = dot(x, wk_ref[...], TN).astype(BF16)
+        for d in (2, 1, 3):
+            send(qkall.at[1, chip], qkall.at[1, chip], sq.at[1], rq.at[1], (kv, along_chips(d)))
         first = iota((16, 2048), 0) == 0
         wsd = jnp.where(first, jnp.broadcast_to(ws_ref[...].astype(F32), (16, 2048)), jnp.broadcast_to(wd_ref[...].astype(F32), (16, 2048)))
-        sdall[tp] = dot(wsd.astype(BF16), x)[0:8]
-    stage_c = []
+        sdall[chip] = dot(wsd.astype(BF16), x)[0:8]
     for d in (2, 1, 3):
         target = (kv, along_chips(d))
-        stage_c.append((send(qkall.at[tp], qkall.at[tp], sq.at[d], rq.at[d], target), send(sdall.at[tp], sdall.at[tp], ssd.at[d], rsd.at[d], target)))
-    stage_m = [send(qkall.at[tp], qkall.at[tp], sqm.at[0], rqm.at[0], (kv, mate)), send(sdall.at[tp], sdall.at[tp], sdm.at[0], rdm.at[0], (kv, mate))]
-    to_mate = send(xnorm, xmate, swm, rwm, (kv, mate))
-    with jax.named_scope("wait_w"):
-        for c in stage_w:
+        send(sdall.at[chip, pl.ds(0, 2)], sdall.at[chip, pl.ds(0, 2)], sq.at[2], rq.at[2], target)
+    stage_c = [total(qkall.at[n, 0:3], sq.at[n], rq.at[n]) for n in range(2)] + [total(sdall.at[0:3, 0:2], sq.at[2], rq.at[2])]
+    with jax.named_scope("wait_wm"):
+        for c in to_mate:
             c.wait_recv()
-    with jax.named_scope("wait_wm"):
-        to_mate.wait_recv()
-    weights = wvz[...].reshape(128, 2048)
-    for h, rows in ((core, xnorm), (1 - core, xmate)):
-        product = dot(weights, rows[...]).astype(BF16).reshape(4, 2, 16, 128)
-        for n in range(4):
-            vzs[n, h] = product[n]
-    stage_v = []
+    product = dot(wvz[...].reshape(256, 2048), xnorm[...]).astype(BF16).reshape(2, 4, 2, 16, 128)
+    for n in range(4):
+        for c in range(2):
+            vzs[n, c] = product[c, n]
     for d in (2, 1, 3):
-        stage_v.append(send(vzs.at[lax.rem(chip + d, 4)], vzall.at[chip], svz.at[d], rvz.at[d], (kv, along_chips(d))))
+        send(vzs.at[lax.rem(chip + d, 4)], vzall.at[chip], svz, rvz, (kv, along_chips(d)))
+    stage_v = [total(vzall.at[0:3], svz, rvz)]
     vzall[chip] = vzs[chip]
     with jax.named_scope("wait_c"):
-        for d, pair in ((1, stage_c[1]), (3, stage_c[2]), (2, stage_c[0])):
-            for c in pair:
-                c.wait_recv()
-            source = lax.rem(chip + 4 - d, 4) * 2 + core
-            stage_m.append(send(qkall.at[source], qkall.at[source], sqm.at[d], rqm.at[d], (kv, mate)))
-            stage_m.append(send(sdall.at[source], sdall.at[source], sdm.at[d], rdm.at[d], (kv, mate)))
-    hgain = jnp.broadcast_to(row_to_column(hgain_ref[...].astype(F32)), (16, 128))
-
-    def reads_of(h):
-        def query_key(m):
-            pieces = [qkall[p * 2 + h, m * 32 : m * 32 + 32, s * 128 : s * 128 + 128] for s in range(2) for p in range(4)]
-            return jnp.concatenate(pieces, axis=0)
-
-        return new_reads(lambda m: abf[pl.ds(pl.multiple_of((h * 4 + m) * 512, 512), 512), :], query_key)
-
-    def half(h, products, offsets):
-        lanes = pl.ds(pl.multiple_of(h * 128, 128), 128)
+        for c in stage_c:
+            c.wait_recv()
+
+    def query_key(m):
+        return jnp.concatenate([qkall[n, p, m * 32 : m * 32 + 32, :] for n in range(2) for p in range(4)], axis=0)
+
+    def accepted_state(m):
+        return abf[pl.ds(pl.multiple_of((core * 4 + m) * 512, 512), 512), :], amate[m * 512 : m * 512 + 512, :]
+
+    with jax.named_scope("reads"):
+        products = new_reads(accepted_state, query_key)
+    with jax.named_scope("wait_v"):
+        for c in stage_v:
+            c.wait_recv()
+    with jax.named_scope("new"):
+        lanes = pl.ds(pl.multiple_of(core * 128, 128), 128)
+        channels = (core, 1 - core)
         outputs = new_part(
             products,
-            [vzall[p, h, 0].astype(F32) for p in range(4)],
-            [sdall[p * 2 + h, 0:1, :] for p in range(4)],
-            [sdall[p * 2 + h, 1:2, :] for p in range(4)],
+            [[vzall[p, c, 0].astype(F32) for p in range(4)] for c in channels],
+            [sdall[p, 0:1, :] for p in range(4)],
+            [sdall[p, 1:2, :] for p in range(4)],
             rate_ref[...],
             [prop_ref[j, :, lanes] for j in range(4)],
             [parent_ref[j : j + 1, lanes] for j in range(4)],
         )
         for p in range(4):
-            o, z = outputs[p], vzall[p, h, 1].astype(F32)
-            sqs[p * 2 + h] = jnp.sum(jnp.square(o), axis=0, keepdims=True)
-            ybuf[p * 2 + h] = (o * hgain * (z * jax.nn.sigmoid(z))).astype(BF16)
-        for o in offsets:
+            sqs[p] = sum_of([jnp.sum(jnp.square(o[p]), axis=0, keepdims=True) for o in outputs])
+            for c, o in zip(channels, outputs):
+                z = vzall[p, c, 1].astype(F32)
+                ybuf[p, c] = (o[p] * hgcol[c] * (z * jax.nn.sigmoid(z))).astype(BF16)
+        place = kv * 4 + chip
+        same_core = far_first(itertools.product(range(4), range(4), range(4), [0]))
+        for o in same_core:
             k, t = device(o)
-            send(sqs.at[t], sqall.at[own], ses, res, (k, t))
-            send(ybuf.at[t], yall.at[core, chip, kv], se, re, (k, t))
-
-    with jax.named_scope("reads1"):
-        products = reads_of(core)
-    with jax.named_scope("wait_v"):
-        for c in stage_v:
+            send(ybuf.at[t // 2], yall.at[chip, kv], se, re, (k, t))
+        for o in same_core:
+            k, t = device(o)
+            send(sqs.at[t // 2], sqall.at[place], ses, res, (k, t))
+    sqall[place] = sqs[chip]
+    yall[chip, kv] = ybuf[chip]
+    with jax.named_scope("wait_o"):
+        for c in stage_o:
             c.wait_recv()
-    with jax.named_scope("new1"):
-        half(core, products, [o for o in everyone if o[3] == 0])
-    sqall[own] = sqs[tp]
-    yall[core, chip, kv] = ybuf[tp]
-    with jax.named_scope("wait_m"):
-        for c in stage_m:
-            c.wait_recv()
-    with jax.named_scope("new2"):
-        half(1 - core, reads_of(1 - core), [o for o in everyone if o[3] == 1])
-    with jax.named_scope("wait_o"):
-        for d, c in ((1, stage_o[1]), (3, stage_o[2]), (2, stage_o[0])):
-            c.wait_recv()
-            block = woall.at[core, lax.rem(chip + 4 - d, 4)]
-            stage_o.append(send(block, block, som.at[3 + d], rom.at[3 + d], (kv, mate)))
-        for c in stage_o[3:]:
-            c.wait_recv()
+        block = woall.at[:, :, core]
+        stage_o.append(send(block, block, som.at[0], rom.at[0], (kv, mate)))
+        stage_o[1].wait_recv()
     with jax.named_scope("wait_e"):
-        all_y, all_sq = total(xall.at[0:2032], se, re), total(sqall.at[0:127], ses, res)
+        all_y, all_sq = total(xall.at[0:2016], se, re), total(sqall.at[0:63], ses, res)
         all_sq.wait_recv()
         all_y.wait_recv()
     with jax.named_scope("combine"):
         for k in range(16):
-            scale = lax.rsqrt(sum_of([sqall[k * 8 + t] for t in range(8)]) / 128.0 + EPS)
+            scale = lax.rsqrt(sum_of([sqall[k * 4 + n] for n in range(4)]) / 128.0 + EPS)
             for c in range(2):
                 for n in range(4):
-                    rows = slice(((c * 4 + n) * 16 + k) * 16, ((c * 4 + n) * 16 + k) * 16 + 16)
-                    ynorm[rows, :] = (yall[c, n, k].astype(F32) * scale).astype(BF16)
+                    rows = slice(((n * 16 + k) * 2 + c) * 16, ((n * 16 + k) * 2 + c) * 16 + 16)
+                    ynorm[rows, :] = (yall[n, k, c].astype(F32) * scale).astype(BF16)
         combined = dot(woall[...].reshape(2048, 128), ynorm[...], TN)
         csend[...] = combined.reshape(8, 16, 128)
         sqf[...] = jnp.sum(jnp.square(combined), axis=0, keepdims=True)
     for o in everyone:
         send(sqf, sums_ref.at[tp * 16 + kv], sh, rh, device(o))
-    stage_f = []
     for b, o in enumerate(line):
         _, t = device(o)
-        stage_f.append(send(csend.at[t], comb_ref.at[tp], sf.at[b], rf.at[b], (kv, t)))
+        send(csend.at[t], comb_ref.at[tp], sf, rf, (kv, t))
     saves.append(pltpu.make_async_copy(sqf, sums_ref.at[tp * 16 + kv], load_sems.at[0]))
     saves.append(pltpu.make_async_copy(csend.at[tp], comb_ref.at[tp], load_sems.at[1]))
     for c in saves[-2:]:
         c.start()
-    sums = total(sqall.at[0:127], sh, rh)
+    stage_f = [total(comb_ref.at[0:7], sf, rf)]
+    sums = total(sums_ref.at[0:127], sh, rh)
     with jax.named_scope("sends"):
-        for pair in stage_c:
-            for c in pair:
-                c.wait_send()
-        for c in list(stage_a.values()) + stage_w + stage_m + stage_v + stage_o + [to_mate, tokens, out_tiles, all_y, all_sq]:
+        for c in list(stage_a.values()) + stage_w + stage_c + stage_v + stage_o + to_mate + [tokens, out_tiles, all_y, all_sq]:
             c.wait_send()
         for c in saves:
             c.wait()
@@ -496,26 +493,27 @@
             *[pltpu.VMEM(a.shape, a.dtype) for a in args],
             pltpu.SemaphoreType.DMA((len(args),)),
             pltpu.VMEM((4096, 128), F32),
-            pltpu.SemaphoreType.DMA((8,)),
+            pltpu.SemaphoreType.DMA(()),
             pltpu.VMEM((2048, 128), BF16),
-            pltpu.VMEM((4, 2, 16, 2048), BF16),
-            pltpu.VMEM((2, 4, 16, 16, 128), BF16),
+            pltpu.VMEM((2, 4, 2, 16, 2048), BF16),
+            pltpu.VMEM((4, 16, 2, 16, 128), BF16),
             pltpu.VMEM((2048, 128), F32),
+            pltpu.VMEM((2, 16, 128), F32),
             pltpu.VMEM((2048, 128), BF16),
             pltpu.VMEM((2048, 128), BF16),
-            pltpu.VMEM((2048, 128), BF16),
-            pltpu.VMEM((8, 128, 256), BF16),
+            pltpu.VMEM((2, 4, 128, 128), BF16),
             pltpu.VMEM((4, 2, 2, 16, 128), BF16),
             pltpu.VMEM((4, 2, 2, 16, 128), BF16),
-            pltpu.VMEM((8, 8, 128), F32),
+            pltpu.VMEM((4, 8, 128), F32),
             pltpu.VMEM((4096, 128), BF16),
-            pltpu.VMEM((8, 16, 128), BF16),
-            pltpu.VMEM((2, 4, 16, 16, 128), BF16),
-            pltpu.VMEM((8, 1, 128), F32),
-            pltpu.VMEM((128, 1, 128), F32),
+            pltpu.VMEM((2048, 128), BF16),
+            pltpu.VMEM((4, 2, 16, 128), BF16),
+            pltpu.VMEM((4, 16, 2, 16, 128), BF16),
+            pltpu.VMEM((4, 1, 128), F32),
+            pltpu.VMEM((64, 1, 128), F32),
             pltpu.VMEM((8, 16, 128), F32),
             pltpu.VMEM((1, 128), F32),
-            *sems(8), *one(), *sems(8), *one(), *sems(4), *sems(4), *sems(4), *sems(4), *sems(4), *one(), *sems(7), *one(), *one(), *sems(8), *one(),
+            *sems(8), *one(), *sems(2), *sems(3), *sems(3), *one(), *one(), *sems(2), *one(), *one(), *one(), *one(),
         ],
         compiler_params=pltpu.CompilerParams(collective_id=0, has_side_effects=True, vmem_limit_bytes=67043328),
     )(*args)

time: 47.3 us -> 46.9 us (level)
  no operation moved by 1% of the time
where the time goes in v5:
time: 46.9 us; the launch traced here: 46.7 us
  Pallas kernels  45.4 us (97%)
  between operations  1.29 us (3%)
    pallas_call x1, Pallas kernels, on_device(): pl.pallas_call(functools.partial(kernel, tp_n, kv_n), out_shape=(jax.Shap...  42.9 us
    pallas_call x1, Pallas kernels, on_device(): pl.pallas_call(finish, out_shape=(jax.ShapeDtypeStruct((4, 16, 256), BF16...  2.53 us

profile of v5, /device:TPU:1, one launch (start us, length us, event | category | flops | bytes accessed | tf_op | source)
XLA Modules:
  0.0 46.7 jit_solution(8719800105148080283)
XLA Ops:
  1.3 42.9 %shard_map.203 = (f32[128,1,128]{2,1,0:T(1,128)}, f32[8,16,128]{2,1,0:T(8,128)}, f32[4096,128]{1,0:T(8,128)}) custom-call(bf16[4,16,256]{2,1,0:T(8,128)(2,1)} %bitcast.36, bf16[16,2048]{1,0:T(8,128)(2,1)} %bitcast.33, bf16[16,2048]{1,0:T(8,128)(2,1)} %bitcast.34, bf16[16,2048]{1,0:T(8,128)(2,1)} %bitcast.35, bf16[16,128]{1,0:T(8,128)(2,1)} %bitcast.40, ...), custom_call_target="tpu_custom_call" | custom-call | tf_op jit(solution)/shard_map/pallas_call | solution.py:483
  44.2 2.5 %shard_map.204 = (bf16[4,16,256]{2,1,0:T(8,128)(2,1)}, f32[4096,128]{1,0:T(8,128)}) custom-call(f32[128,1,128]{2,1,0:T(1,128)} %get-tuple-element.7.sums_in, f32[8,16,128]{2,1,0:T(8,128)} %get-tuple-element.8.comb_in, bf16[1,16]{1,0:T(2,128)(2,1)} %bitcast.47, f32[4096,128]{1,0:T(8,128)} %get-tuple-element.9.acc_in), custom_call_target="tpu_custom_call" | custom-call | tf_op jit(solution)/shard_map/pallas_call | solution.py:520

commit v6 on v5

--- a/solution.py
+++ b/solution.py
@@ -231,11 +231,10 @@
             send(xall.at[rows], xall.at[rows], st, rt, device(o))
 
     own_rows = pl.ds(pl.multiple_of(own * 16, 16), 16)
-    stage_a = {}
     with jax.named_scope("issue_t"):
-        for b, o in enumerate(line):
+        for o in line:
             _, t = device(o)
-            stage_a[o[2:]] = send(xt_ref.at[t // 2, :, lanes_of(t)], xall.at[own_rows], sa.at[b], ra.at[b], (kv, t))
+            send(xt_ref.at[t // 2, :, lanes_of(t)], xall.at[own_rows], sa.at[o[2]], ra.at[o[2]], (kv, t))
         xall[own_rows, :] = xt_ref[tp // 2, :, lanes_of(tp)]
         own_tile = xt_ref.at[tp // 2, :, lanes_of(tp)]
         for o in plane:
@@ -259,11 +258,11 @@
         gaincol[n * 128 : n * 128 + 128, :] = jnp.broadcast_to(column, (128, 128))
     hgcol[core] = jnp.broadcast_to(row_to_column(hgain_ref[...].astype(F32)), (16, 128))
     with jax.named_scope("wait_a"):
-        stage_a[0, 1].wait_recv()
+        stage_a = {d: total(xall.at[0 : 32 if d else 16], sa.at[d], ra.at[d]) for d in range(4)}
+        stage_a[0].wait_recv()
         hand_on(mate, 1)
         for d in (1, 3, 2):
-            for c in range(2):
-                stage_a[d, c].wait_recv()
+            stage_a[d].wait_recv()
             hand_on(lax.rem(chip + 4 - d, 4) * 2, 2)
     tokens = total(xall.at[0:1920], st, rt)
     for c in loads[5:18]:
@@ -423,11 +422,11 @@
 
 def finish(sums_in, comb_in, gain_in, acc_in, out_ref, acc_ref, sums, comb, gain, outv, accv, loaded, saved):
     pieces = [(sums_in, sums), (comb_in, comb), (gain_in, gain)]
-    blocks = [pl.ds(g * 512, 512) for g in range(8)]
+    blocks = [pl.ds(g * 1024, 1024) for g in range(4)]
     pieces += [(acc_in.at[rows], accv.at[rows]) for rows in blocks]
     loads = [pltpu.make_async_copy(a, b, loaded.at[n]) for n, (a, b) in enumerate(pieces)]
-    saves = [pltpu.make_async_copy(accv.at[rows], acc_ref.at[rows], saved.at[g]) for g, rows in enumerate(blocks)]
-    saves.append(pltpu.make_async_copy(outv, out_ref, saved.at[8]))
+    saves = [pltpu.make_async_copy(accv.at[rows], acc_ref.at[rows], saved.at[0]) for rows in blocks]
+    last = pltpu.make_async_copy(outv, out_ref, saved.at[1])
     for c in loads:
         c.start()
     for c in loads[:3]:
@@ -436,12 +435,12 @@
     for t in range(8):
         scale = lax.rsqrt(sum_of([sums[t * 16 + k] for k in range(16)]) / 2048.0 + EPS)
         outv[t // 2, :, (t % 2) * 128 : (t % 2) * 128 + 128] = (comb[t] * scale * column).astype(BF16)
-    saves[8].start()
+    last.start()
     for load, save in zip(loads[3:], saves):
         load.wait()
         save.start()
-    for c in saves:
-        c.wait()
+    pltpu.make_async_copy(accv, acc_ref, saved.at[0]).wait()
+    last.wait()
 
 
 def on_device(
@@ -513,7 +512,7 @@
             pltpu.VMEM((64, 1, 128), F32),
             pltpu.VMEM((8, 16, 128), F32),
             pltpu.VMEM((1, 128), F32),
-            *sems(8), *one(), *sems(2), *sems(3), *sems(3), *one(), *one(), *sems(2), *one(), *one(), *one(), *one(),
+            *sems(4), *one(), *sems(2), *sems(3), *sems(3), *one(), *one(), *sems(2), *one(), *one(), *one(), *one(),
         ],
         compiler_params=pltpu.CompilerParams(collective_id=0, has_side_effects=True, vmem_limit_bytes=67043328),
     )(*args)
@@ -528,8 +527,8 @@
             pltpu.VMEM((1, 16), BF16),
             pltpu.VMEM((4, 16, 256), BF16),
             pltpu.VMEM((4096, 128), F32),
-            pltpu.SemaphoreType.DMA((11,)),
-            pltpu.SemaphoreType.DMA((9,)),
+            pltpu.SemaphoreType.DMA((7,)),
+            pltpu.SemaphoreType.DMA((2,)),
         ],
         compiler_params=pltpu.CompilerParams(vmem_limit_bytes=67043328),
     )(sums, combined, output_norm_gain.reshape(1, 16), acc)

time: 46.9 us -> 46.8 us (level)
  no operation moved by 1% of the time
where the time goes in v6:
time: 46.8 us; the launch traced here: 46.7 us
  Pallas kernels  45.4 us (97%)
  between operations  1.29 us (3%)
    pallas_call x1, Pallas kernels, on_device(): pl.pallas_call(functools.partial(kernel, tp_n, kv_n), out_shape=(jax.Shap...  42.8 us
    pallas_call x1, Pallas kernels, on_device(): pl.pallas_call(finish, out_shape=(jax.ShapeDtypeStruct((4, 16, 256), BF16...  2.53 us

profile of v6, /device:TPU:1, one launch (start us, length us, event | category | flops | bytes accessed | tf_op | source)
XLA Modules:
  0.0 46.7 jit_solution(5355393494055988637)
XLA Ops:
  1.3 42.8 %shard_map.203 = (f32[128,1,128]{2,1,0:T(1,128)}, f32[8,16,128]{2,1,0:T(8,128)}, f32[4096,128]{1,0:T(8,128)}) custom-call(bf16[4,16,256]{2,1,0:T(8,128)(2,1)} %bitcast.36, bf16[16,2048]{1,0:T(8,128)(2,1)} %bitcast.33, bf16[16,2048]{1,0:T(8,128)(2,1)} %bitcast.34, bf16[16,2048]{1,0:T(8,128)(2,1)} %bitcast.35, bf16[16,128]{1,0:T(8,128)(2,1)} %bitcast.40, ...), custom_call_target="tpu_custom_call" | custom-call | tf_op jit(solution)/shard_map/pallas_call | solution.py:482
  44.1 2.5 %shard_map.204 = (bf16[4,16,256]{2,1,0:T(8,128)(2,1)}, f32[4096,128]{1,0:T(8,128)}) custom-call(f32[128,1,128]{2,1,0:T(1,128)} %get-tuple-element.7.sums_in, f32[8,16,128]{2,1,0:T(8,128)} %get-tuple-element.8.comb_in, bf16[1,16]{1,0:T(2,128)(2,1)} %bitcast.47, f32[4096,128]{1,0:T(8,128)} %get-tuple-element.9.acc_in), custom_call_target="tpu_custom_call" | custom-call | tf_op jit(solution)/shard_map/pallas_call | solution.py:519
